TPU v7x, 32 devices: a whole 2x2x4 slice. The times are simulated.
32 devices in a mesh: gr: 2 (over y), sp: 4 (over z), tp: 4 (over x, core).
Axes of the slice: x: 2, y: 2, z: 4, core: 2. Of those that a mesh axis runs over, the one named last changes fastest.
Arguments:
- layer_input: bfloat16 [2, 3072, 2048], P('gr', ('sp', 'tp')), may hold values from -6 to 6
- key_weight: bfloat16 [2048, 2048], P(None, 'tp'), may hold values from -0.125 to 0.125
- value_weight: bfloat16 [2048, 2048], P(None, 'tp'), may hold values from -0.125 to 0.125
- new_queries: bfloat16 [2, 2048], P('gr', 'tp'), may hold values from -280 to 280
- lambdas: float32 [16], P('tp'), may hold values from 0.3 to 0.8
- head_gain: float32 [128], replicated, may hold values from 0.1 to 1.9
- out_weight: bfloat16 [2048, 2048], P('tp'), may hold values from -0.125 to 0.125
Outputs:
- key_cache: bfloat16 [2, 3072, 2048], P('gr', 'sp', 'tp')
- value_cache: bfloat16 [2, 3072, 2048], P('gr', 'sp', 'tp')
- mixed: bfloat16 [2, 2048], P('gr', 'tp')
All inputs are finite; a program needn't handle non-finite values.
Results may differ from a plain program's by a relative error of at most 0.03.
Values may be sent and summed in bfloat16 or wider, within the bound.
A program may use at most 64 MiB of HBM per device.

v0:
```python
import functools

import jax
import jax.numpy as jnp
import numpy as np
from jax import lax
from jax.experimental import pallas as pl
from jax.experimental.pallas import tpu as pltpu
from jax.sharding import PartitionSpec as P

MESH = pl.DeviceIdType.MESH
MAP_ROWS = 16
VMEM_BYTES = 67043328
SMALL_BYTES = 16384


def kernel(
    n_sp, n_tp, heads, head_dim, chunk,
    x_ref, wk_ref, wv_ref, q_ref, lam_ref, gain_ref, wo_ref, fine_ref, coarse_ref,
    keys, values, mix_ref,
    xg, wk, wv, wo, q, lam, gain, fine, coarse, stats, part, parts,
    load_sem, up_sem, down_sem, near_send, near_recv, far_send, far_recv, fwd_send, fwd_recv,
    st_send, st_recv, pt_send, pt_recv,
):
    sp = lax.axis_index("sp")
    tp = lax.axis_index("tp")
    rows = x_ref.shape[1]
    wide = 2 * head_dim
    maps = 2 * heads
    steps = rows // chunk
    chips = n_tp // 2
    partner = tp + 1 - 2 * lax.rem(tp, 2)
    out_cols = mix_ref.shape[1]
    local_coarse = n_tp * steps

    own_load = pltpu.make_async_copy(x_ref.at[0], xg.at[tp], load_sem.at[0])
    loads = [
        pltpu.make_async_copy(q_ref, q, load_sem.at[5]),
        pltpu.make_async_copy(wk_ref, wk, load_sem.at[1]),
        pltpu.make_async_copy(wv_ref, wv, load_sem.at[2]),
        pltpu.make_async_copy(fine_ref, fine, load_sem.at[3]),
        pltpu.make_async_copy(
            coarse_ref.at[pl.ds(sp * local_coarse, local_coarse)], coarse, load_sem.at[4]
        ),
        pltpu.make_async_copy(lam_ref, lam, load_sem.at[6]),
        pltpu.make_async_copy(gain_ref, gain, load_sem.at[7]),
        pltpu.make_async_copy(wo_ref, wo, load_sem.at[8]),
    ]

    own_load.start()
    barrier = pltpu.get_barrier_semaphore()
    for d in range(1, n_tp):
        pl.semaphore_signal(
            barrier, inc=1, device_id={"tp": lax.rem(tp + d, n_tp)}, device_id_type=MESH
        )
    has_lower = sp > 0
    has_upper = sp < n_sp - 1

    @pl.when(has_lower)
    def _():
        pl.semaphore_signal(barrier, inc=1, device_id={"sp": sp - 1}, device_id_type=MESH)

    @pl.when(has_upper)
    def _():
        pl.semaphore_signal(barrier, inc=1, device_id={"sp": sp + 1}, device_id_type=MESH)

    pl.semaphore_wait(barrier, n_tp - 1 + jnp.where(has_lower, 1, 0) + jnp.where(has_upper, 1, 0))

    own_load.wait()
    far = {}
    for j in range(steps):
        for d in range(1, chips):
            far[d, j] = pltpu.make_async_remote_copy(
                src_ref=xg.at[tp, pl.ds(j * chunk, chunk)],
                dst_ref=xg.at[tp, pl.ds(j * chunk, chunk)],
                send_sem=far_send.at[d - 1, j],
                recv_sem=far_recv.at[d - 1, j],
                device_id={"tp": lax.rem(tp + 2 * d, n_tp)},
                device_id_type=MESH,
            )
            far[d, j].start()
    near = pltpu.make_async_remote_copy(
        src_ref=xg.at[tp],
        dst_ref=xg.at[tp],
        send_sem=near_send,
        recv_sem=near_recv,
        device_id={"tp": partner},
        device_id_type=MESH,
    )
    for load in loads:
        load.start()
    near.start()

    pl.when(has_lower)(lambda: pl.semaphore_wait(up_sem, 1))

    @pl.when(has_upper)
    def _():
        pl.semaphore_signal(up_sem, inc=1, device_id={"sp": sp + 1}, device_id_type=MESH)
        pl.semaphore_wait(down_sem, 1)

    @pl.when(has_lower)
    def _():
        pl.semaphore_signal(down_sem, inc=1, device_id={"sp": sp - 1}, device_id_type=MESH)

    lane = lax.broadcasted_iota(jnp.int32, (chunk, wide), 1)
    low_half = lax.rem(lane, head_dim) < head_dim // 2

    def project(block, first, count):
        piece = xg[block, first * chunk:(first + count) * chunk, :]
        raw_keys = jnp.dot(piece, wk[...], preferred_element_type=jnp.float32)
        raw_values = jnp.dot(piece, wv[...], preferred_element_type=jnp.float32)
        values[block, first * chunk:(first + count) * chunk, :] = raw_values.astype(jnp.bfloat16)
        for i in range(count):
            base = coarse[block * steps + first + i]
            base_cos, base_sin = base[0:1, :], base[1:2, :]
            cosine = base_cos * fine[0] - base_sin * fine[1]
            sine = base_sin * fine[0] + base_cos * fine[1]
            for h in range(heads):
                raw = raw_keys[i * chunk:(i + 1) * chunk, h * wide:(h + 1) * wide]
                ahead = pltpu.roll(raw, wide - head_dim // 2, 1)
                behind = pltpu.roll(raw, head_dim // 2, 1)
                turned = raw * cosine + jnp.where(low_half, ahead, behind) * sine
                keys[
                    block, (first + i) * chunk:(first + i + 1) * chunk, h * wide:(h + 1) * wide
                ] = turned.astype(jnp.bfloat16)

    for load in loads[:5]:
        load.wait()
    map_row = lax.broadcasted_iota(jnp.int32, (MAP_ROWS, q.shape[1]), 0)
    map_col = lax.broadcasted_iota(jnp.int32, (MAP_ROWS, q.shape[1]), 1) // head_dim
    spread = jnp.where(map_row == map_col, q[...].astype(jnp.float32), 0.0).astype(jnp.bfloat16)

    def attend(state, block, first, count):
        where = slice(first * chunk, (first + count) * chunk)
        score = lax.dot_general(
            spread, keys[block, where, :], (((1,), (1,)), ((), ())),
            preferred_element_type=jnp.float32,
        ) * head_dim ** (-0.5)
        highest = jnp.max(score, axis=1, keepdims=True)
        if state is not None:
            highest = jnp.maximum(highest, state[0])
        weight = jnp.exp(score - highest)
        total = jnp.sum(weight, axis=1, keepdims=True)
        upper = weight.astype(jnp.bfloat16)
        lower = (weight - upper.astype(jnp.float32)).astype(jnp.bfloat16)
        read = jnp.dot(
            jnp.concatenate([upper, lower], axis=0), values[block, where, :],
            preferred_element_type=jnp.float32,
        )
        read = read[:MAP_ROWS] + read[MAP_ROWS:]
        if state is not None:
            fade = jnp.exp(state[0] - highest)
            total = total + state[1] * fade
            read = read + state[2] * fade
        return highest, total, read

    project(tp, 0, steps)
    state = attend(None, tp, 0, steps)
    near.wait_recv()
    project(partner, 0, steps)
    state = attend(state, partner, 0, steps)

    forwards = []
    for j in range(steps):
        for d in range(1, chips):
            source = lax.rem(tp + n_tp - 2 * d, n_tp)
            other = source + 1 - 2 * lax.rem(source, 2)
            far[d, j].wait_recv()
            forward = pltpu.make_async_remote_copy(
                src_ref=xg.at[source, pl.ds(j * chunk, chunk)],
                dst_ref=xg.at[source, pl.ds(j * chunk, chunk)],
                send_sem=fwd_send.at[d - 1, j],
                recv_sem=fwd_recv.at[d - 1, j],
                device_id={"tp": partner},
                device_id_type=MESH,
            )
            forward.start()
            forwards.append(forward)
            project(source, j, 1)
            state = attend(state, source, j, 1)
            forward.wait_recv()
            project(other, j, 1)
            state = attend(state, other, j, 1)

    for load in loads[5:]:
        load.wait()
    highest, total, read = state
    head_of = lax.broadcasted_iota(jnp.int32, (MAP_ROWS, wide), 0) // 2
    own = jnp.zeros((MAP_ROWS, wide), jnp.float32)
    for h in range(heads):
        own = jnp.where(head_of == h, read[:, h * wide:(h + 1) * wide], own)
    first_lane = lax.broadcasted_iota(jnp.int32, (MAP_ROWS, wide), 1) == 0
    stats[sp, 0] = own[:maps]
    stats[sp, 1] = jnp.where(first_lane, highest, total)[:maps]

    exchanges = []
    for d in range(n_sp - 1, 0, -1):
        copy = pltpu.make_async_remote_copy(
            src_ref=stats.at[sp],
            dst_ref=stats.at[sp],
            send_sem=st_send.at[d - 1],
            recv_sem=st_recv.at[d - 1],
            device_id={"sp": lax.rem(sp + d, n_sp)},
            device_id_type=MESH,
        )
        copy.start()
        exchanges.append(copy)
    for copy in exchanges:
        copy.wait_recv()
    heights = stats[:, 1]
    tops = heights[:, :, 0:1]
    sums = heights[:, :, 1:2]
    factor = jnp.exp(tops - jnp.max(tops, axis=0, keepdims=True))
    totals = jnp.sum(sums * factor, axis=0)
    reads = jnp.sum(stats[:, 0] * factor, axis=0) / totals
    normed = []
    for h in range(heads):
        diff = reads[2 * h:2 * h + 1] - lam[0:1, h:h + 1] * reads[2 * h + 1:2 * h + 2]
        scale = lax.rsqrt(jnp.mean(diff * diff, axis=1, keepdims=True) + 1e-06)
        normed.append(diff * scale * gain[...])
    headed = jnp.concatenate(normed, axis=1)
    headed = jnp.broadcast_to(headed, (MAP_ROWS, headed.shape[1])).astype(jnp.bfloat16)
    partials = jnp.dot(headed, wo[...], preferred_element_type=jnp.float32).astype(jnp.bfloat16)
    for b in range(n_tp):
        part[b] = partials[:, b * out_cols:(b + 1) * out_cols]
    swaps = []
    for d in range(n_tp - 1, 0, -1):
        target = lax.rem(tp + d, n_tp)
        copy = pltpu.make_async_remote_copy(
            src_ref=part.at[target],
            dst_ref=parts.at[d - 1],
            send_sem=pt_send.at[d - 1],
            recv_sem=pt_recv.at[d - 1],
            device_id={"tp": target},
            device_id_type=MESH,
        )
        copy.start()
        swaps.append(copy)
    mixed = part[tp].astype(jnp.float32)
    for copy in swaps:
        copy.wait_recv()
    for d in range(1, n_tp):
        mixed = mixed + parts[d - 1].astype(jnp.float32)
    mix_ref[...] = mixed[0:1].astype(jnp.bfloat16)

    near.wait_send()
    for copy in list(far.values()) + forwards + exchanges + swaps:
        copy.wait_send()


def tables(length, chunk, head_dim):
    inverse = 1.0 / 10000.0 ** (np.arange(0, head_dim, 2) / head_dim)
    inverse = np.tile(inverse, 4)
    sign = np.tile(np.repeat([-1.0, 1.0], head_dim // 2), 2)

    def pair(positions, axis):
        angles = positions[:, None] * inverse[None, :]
        both = np.stack([np.cos(angles), np.sin(angles) * sign], axis=axis)
        return both.astype(np.float32)

    return pair(np.arange(chunk), 0), pair(np.arange(0, length, chunk), 1)


def on_device(n_sp, n_tp, x, key_weight, value_weight, new_queries, lambdas, head_gain, out_weight):
    heads = lambdas.shape[0]
    columns = key_weight.shape[1]
    head_dim = columns // (2 * heads)
    wide = 2 * head_dim
    seqs, rows, depth = x.shape
    assert seqs == 1
    chunk = rows // 4
    steps = rows // chunk
    chips = n_tp // 2
    out_cols = out_weight.shape[1] // n_tp
    fine, coarse = tables(n_sp * n_tp * rows, chunk, head_dim)
    hbm_spec = pl.BlockSpec(memory_space=pltpu.HBM)
    dma = pltpu.SemaphoreType.DMA
    bf16 = jnp.bfloat16
    f32 = jnp.float32
    room = 2 * n_tp * rows * columns * 2 + SMALL_BYTES
    k, v, mixed = pl.pallas_call(
        functools.partial(kernel, n_sp, n_tp, heads, head_dim, chunk),
        out_shape=(
            pltpu.VMEM((n_tp, rows, columns), bf16),
            pltpu.VMEM((n_tp, rows, columns), bf16),
            jax.ShapeDtypeStruct((1, out_cols), bf16),
        ),
        in_specs=[hbm_spec] * 9,
        out_specs=(pl.BlockSpec(memory_space=pltpu.VMEM),) * 3,
        scratch_shapes=[
            pltpu.VMEM((n_tp, rows, depth), bf16),
            pltpu.VMEM((depth, columns), bf16),
            pltpu.VMEM((depth, columns), bf16),
            pltpu.VMEM(out_weight.shape, bf16),
            pltpu.VMEM((1, columns), bf16),
            pltpu.VMEM((1, heads), f32),
            pltpu.VMEM((1, wide), f32),
            pltpu.VMEM((2, chunk, wide), f32),
            pltpu.VMEM((n_tp * steps, 2, wide), f32),
            pltpu.VMEM((n_sp, 2, 2 * heads, wide), f32),
            pltpu.VMEM((n_tp, MAP_ROWS, out_cols), bf16),
            pltpu.VMEM((n_tp - 1, MAP_ROWS, out_cols), bf16),
            dma((9,)),
            pltpu.SemaphoreType.REGULAR,
            pltpu.SemaphoreType.REGULAR,
            dma,
            dma,
            dma((chips - 1, steps)),
            dma((chips - 1, steps)),
            dma((chips - 1, steps)),
            dma((chips - 1, steps)),
            dma((n_sp - 1,)),
            dma((n_sp - 1,)),
            dma((n_tp - 1,)),
            dma((n_tp - 1,)),
        ],
        compiler_params=pltpu.CompilerParams(
            collective_id=0, has_side_effects=True, vmem_limit_bytes=VMEM_BYTES - room
        ),
    )(
        x, key_weight, value_weight, new_queries, lambdas.reshape(1, heads),
        head_gain.reshape(1, wide), out_weight, jnp.asarray(fine), jnp.asarray(coarse),
    )
    full = (1, n_tp * rows, columns)
    return k.reshape(full), v.reshape(full), mixed


def solution(mesh):
    n_sp, n_tp = mesh.shape["sp"], mesh.shape["tp"]
    in_specs = (
        P("gr", ("sp", "tp"), None),
        P(None, "tp"),
        P(None, "tp"),
        P("gr", "tp"),
        P("tp"),
        P(),
        P("tp", None),
    )
    out_specs = (P("gr", "sp", "tp"), P("gr", "sp", "tp"), P("gr", "tp"))
    return jax.shard_map(
        functools.partial(on_device, n_sp, n_tp),
        mesh=mesh, in_specs=in_specs, out_specs=out_specs, check_vma=False,
    )
```

profile of v0, /device:TPU:0, one launch (start us, length us, event | category | flops | bytes accessed | tf_op | source)
XLA Modules:
  0.0 36.9 jit_solution(2789621203862307661)
XLA Ops:
  0.6 33.9 %shard_map.112 = (bf16[4,192,512]{2,1,0:T(8,128)(2,1)S(1)}, bf16[4,192,512]{2,1,0:T(8,128)(2,1)S(1)}, bf16[1,512]{1,0:T(2,128)(2,1)}) custom-call(bf16[1,192,2048]{2,1,0:T(8,128)(2,1)} %x_ref.1, bf16[2048,512]{1,0:T(8,128)(2,1)} %wk_ref.1, bf16[2048,512]{1,0:T(8,128)(2,1)} %wv_ref.1, bf16[1,512]{1,0:T(2,128)(2,1)} %q_ref.1, f32[1,4]{1,0:T(1,128)} %bitcast.6, ...), custom_call_target="tpu_custom_call" | custom-call | tf_op jit(solution)/shard_map/pallas_call | solution.py:281
  34.5 0.0 copy-start
  34.5 0.9 %copy.15 = bf16[1,768,512]{2,1,0:T(8,128)(2,1)} copy(bf16[1,768,512]{2,1,0:T(8,128)(2,1)S(1)} %bitcast.5) | data formatting | bytes 1572864
  35.4 0.9 %copy.16 = bf16[1,768,512]{2,1,0:T(8,128)(2,1)} copy(bf16[1,768,512]{2,1,0:T(8,128)(2,1)S(1)} %bitcast.4) | data formatting | bytes 1572864
  36.3 0.0 copy-done
  36.3 0.6 %copy.17 = bf16[1,512]{1,0:T(2,128)(2,1)} copy(bf16[1,512]{1,0:T(2,128)(2,1)S(1)} %copy-done) | data formatting | bytes 2048
Async XLA Ops:
  34.5 1.8 %copy-start = (bf16[1,512]{1,0:T(2,128)(2,1)S(1)}, bf16[1,512]{1,0:T(2,128)(2,1)}, u32[]{:S(2)}) copy-start(bf16[1,512]{1,0:T(2,128)(2,1)} %get-tuple-element.17) | copy-start | bytes 3076
where the time goes:
time: 37 us; the launch traced here: 36.9 us
  Pallas kernels  33.9 us (92%)
  local copies, waits for them, and re-layouts  2.34 us (6%)
  between operations  0.65 us (2%)
    pallas_call x1, Pallas kernels, on_device(): pl.pallas_call(functools.partial(kernel, n_sp, n_tp, heads, head_dim, chu...  33.9 us
    unnamed x5, local copies, waits for them, and re-layouts  2.34 us

commit v1 on v0

--- a/solution.py
+++ b/solution.py
@@ -12,19 +12,21 @@
 MAP_ROWS = 16
 VMEM_BYTES = 67043328
 SMALL_BYTES = 16384
+SLICES = (3, 2, 2, 1)
 
 
 def kernel(
     n_sp, n_tp, heads, head_dim, chunk,
     x_ref, wk_ref, wv_ref, q_ref, lam_ref, gain_ref, wo_ref, fine_ref, coarse_ref,
     keys, values, mix_ref,
-    xg, wk, wv, wo, q, lam, gain, fine, coarse, stats, part, parts,
-    load_sem, up_sem, down_sem, near_send, near_recv, far_send, far_recv, fwd_send, fwd_recv,
+    xg, wk, wv, wo, q, lam, gain, fine, coarse, stats, part, parts, sums,
+    load_sem, own_sem, up_sem, down_sem, near_send, near_recv, far_send, far_recv, fwd_send, fwd_recv,
     st_send, st_recv, pt_send, pt_recv,
 ):
     sp = lax.axis_index("sp")
     tp = lax.axis_index("tp")
-    rows = x_ref.shape[1]
+    rows, depth = x_ref.shape[1:]
+    columns = wk.shape[1]
     wide = 2 * head_dim
     maps = 2 * heads
     steps = rows // chunk
@@ -32,8 +34,22 @@
     partner = tp + 1 - 2 * lax.rem(tp, 2)
     out_cols = mix_ref.shape[1]
     local_coarse = n_tp * steps
-
-    own_load = pltpu.make_async_copy(x_ref.at[0], xg.at[tp], load_sem.at[0])
+    last = steps - 1
+    unit = depth // sum(SLICES)
+    edges = [unit * sum(SLICES[:i]) for i in range(len(SLICES) + 1)]
+    cuts = [slice(edges[i], edges[i + 1]) for i in range(len(SLICES))]
+    pieces = [(j, slice(0, depth)) for j in range(last)] + [(last, cut) for cut in cuts]
+
+    def piece_of(block, piece):
+        j, cut = pieces[piece]
+        return xg.at[block, pl.ds(j * chunk, chunk), pl.ds(cut.start, cut.stop - cut.start)]
+
+    own_loads = [
+        pltpu.make_async_copy(
+            x_ref.at[0, pl.ds(j * chunk, chunk)], xg.at[tp, pl.ds(j * chunk, chunk)], own_sem.at[j]
+        )
+        for j in range(steps)
+    ]
     loads = [
         pltpu.make_async_copy(q_ref, q, load_sem.at[5]),
         pltpu.make_async_copy(wk_ref, wk, load_sem.at[1]),
@@ -47,7 +63,6 @@
         pltpu.make_async_copy(wo_ref, wo, load_sem.at[8]),
     ]
 
-    own_load.start()
     barrier = pltpu.get_barrier_semaphore()
     for d in range(1, n_tp):
         pl.semaphore_signal(
@@ -64,21 +79,24 @@
     def _():
         pl.semaphore_signal(barrier, inc=1, device_id={"sp": sp + 1}, device_id_type=MESH)
 
+    for load in own_loads:
+        load.start()
     pl.semaphore_wait(barrier, n_tp - 1 + jnp.where(has_lower, 1, 0) + jnp.where(has_upper, 1, 0))
 
-    own_load.wait()
     far = {}
-    for j in range(steps):
+    for p in range(len(pieces)):
+        if p < steps:
+            own_loads[p].wait()
         for d in range(1, chips):
-            far[d, j] = pltpu.make_async_remote_copy(
-                src_ref=xg.at[tp, pl.ds(j * chunk, chunk)],
-                dst_ref=xg.at[tp, pl.ds(j * chunk, chunk)],
-                send_sem=far_send.at[d - 1, j],
-                recv_sem=far_recv.at[d - 1, j],
+            far[d, p] = pltpu.make_async_remote_copy(
+                src_ref=piece_of(tp, p),
+                dst_ref=piece_of(tp, p),
+                send_sem=far_send.at[d - 1, p],
+                recv_sem=far_recv.at[d - 1, p],
                 device_id={"tp": lax.rem(tp + 2 * d, n_tp)},
                 device_id_type=MESH,
             )
-            far[d, j].start()
+            far[d, p].start()
     near = pltpu.make_async_remote_copy(
         src_ref=xg.at[tp],
         dst_ref=xg.at[tp],
@@ -87,28 +105,14 @@
         device_id={"tp": partner},
         device_id_type=MESH,
     )
+    near.start()
     for load in loads:
         load.start()
-    near.start()
-
-    pl.when(has_lower)(lambda: pl.semaphore_wait(up_sem, 1))
-
-    @pl.when(has_upper)
-    def _():
-        pl.semaphore_signal(up_sem, inc=1, device_id={"sp": sp + 1}, device_id_type=MESH)
-        pl.semaphore_wait(down_sem, 1)
-
-    @pl.when(has_lower)
-    def _():
-        pl.semaphore_signal(down_sem, inc=1, device_id={"sp": sp - 1}, device_id_type=MESH)
 
     lane = lax.broadcasted_iota(jnp.int32, (chunk, wide), 1)
     low_half = lax.rem(lane, head_dim) < head_dim // 2
 
-    def project(block, first, count):
-        piece = xg[block, first * chunk:(first + count) * chunk, :]
-        raw_keys = jnp.dot(piece, wk[...], preferred_element_type=jnp.float32)
-        raw_values = jnp.dot(piece, wv[...], preferred_element_type=jnp.float32)
+    def settle(block, first, count, raw_keys, raw_values):
         values[block, first * chunk:(first + count) * chunk, :] = raw_values.astype(jnp.bfloat16)
         for i in range(count):
             base = coarse[block * steps + first + i]
@@ -124,10 +128,19 @@
                     block, (first + i) * chunk:(first + i + 1) * chunk, h * wide:(h + 1) * wide
                 ] = turned.astype(jnp.bfloat16)
 
+    def product(block, first, count, cut):
+        piece = xg[block, first * chunk:(first + count) * chunk, cut]
+        raw_keys = jnp.dot(piece, wk[cut, :], preferred_element_type=jnp.float32)
+        raw_values = jnp.dot(piece, wv[cut, :], preferred_element_type=jnp.float32)
+        return raw_keys, raw_values
+
+    def project(block, first, count):
+        settle(block, first, count, *product(block, first, count, slice(0, depth)))
+
     for load in loads[:5]:
         load.wait()
-    map_row = lax.broadcasted_iota(jnp.int32, (MAP_ROWS, q.shape[1]), 0)
-    map_col = lax.broadcasted_iota(jnp.int32, (MAP_ROWS, q.shape[1]), 1) // head_dim
+    map_row = lax.broadcasted_iota(jnp.int32, (MAP_ROWS, columns), 0)
+    map_col = lax.broadcasted_iota(jnp.int32, (MAP_ROWS, columns), 1) // head_dim
     spread = jnp.where(map_row == map_col, q[...].astype(jnp.float32), 0.0).astype(jnp.bfloat16)
 
     def attend(state, block, first, count):
@@ -156,34 +169,83 @@
 
     project(tp, 0, steps)
     state = attend(None, tp, 0, steps)
+
+    pl.when(has_lower)(lambda: pl.semaphore_wait(up_sem, 1))
+
+    @pl.when(has_upper)
+    def _():
+        pl.semaphore_signal(up_sem, inc=1, device_id={"sp": sp + 1}, device_id_type=MESH)
+
     near.wait_recv()
     project(partner, 0, steps)
     state = attend(state, partner, 0, steps)
 
-    forwards = []
-    for j in range(steps):
-        for d in range(1, chips):
-            source = lax.rem(tp + n_tp - 2 * d, n_tp)
-            other = source + 1 - 2 * lax.rem(source, 2)
-            far[d, j].wait_recv()
-            forward = pltpu.make_async_remote_copy(
-                src_ref=xg.at[source, pl.ds(j * chunk, chunk)],
-                dst_ref=xg.at[source, pl.ds(j * chunk, chunk)],
-                send_sem=fwd_send.at[d - 1, j],
-                recv_sem=fwd_recv.at[d - 1, j],
-                device_id={"tp": partner},
-                device_id_type=MESH,
-            )
-            forward.start()
-            forwards.append(forward)
-            project(source, j, 1)
-            state = attend(state, source, j, 1)
-            forward.wait_recv()
-            project(other, j, 1)
-            state = attend(state, other, j, 1)
+    pl.when(has_upper)(lambda: pl.semaphore_wait(down_sem, 1))
+
+    @pl.when(has_lower)
+    def _():
+        pl.semaphore_signal(down_sem, inc=1, device_id={"sp": sp - 1}, device_id_type=MESH)
 
     for load in loads[5:]:
         load.wait()
+    map_of = lax.broadcasted_iota(jnp.int32, (maps, wide), 0)
+    lam_row = jnp.zeros((maps, wide), jnp.float32)
+    for h in range(heads):
+        lam_row = jnp.where(map_of == 2 * h, lam[0:1, h:h + 1], lam_row)
+
+    sources = {d: lax.rem(tp + n_tp - 2 * d, n_tp) for d in range(1, chips)}
+    others = {d: sources[d] + 1 - 2 * lax.rem(sources[d], 2) for d in sources}
+    forwards = {}
+
+    def forward(d, p):
+        far[d, p].wait_recv()
+        forwards[d, p] = pltpu.make_async_remote_copy(
+            src_ref=piece_of(sources[d], p),
+            dst_ref=piece_of(sources[d], p),
+            send_sem=fwd_send.at[d - 1, p],
+            recv_sem=fwd_recv.at[d - 1, p],
+            device_id={"tp": partner},
+            device_id_type=MESH,
+        )
+        forwards[d, p].start()
+
+    for j in range(last):
+        for d in sources:
+            forward(d, j)
+            project(sources[d], j, 1)
+            state = attend(state, sources[d], j, 1)
+            forwards[d, j].wait_recv()
+            project(others[d], j, 1)
+            state = attend(state, others[d], j, 1)
+
+    def add_slice(d, side, block, i):
+        raw_keys, raw_values = product(block, last, 1, cuts[i])
+        slot = 2 * (d - 1) + side
+        if i > 0:
+            raw_keys = raw_keys + sums[slot, :, :columns]
+            raw_values = raw_values + sums[slot, :, columns:]
+        if i < len(cuts) - 1:
+            sums[slot, :, :columns] = raw_keys
+            sums[slot, :, columns:] = raw_values
+        else:
+            settle(block, last, 1, raw_keys, raw_values)
+
+    final = len(cuts) - 1
+    for i in range(len(cuts)):
+        for d in sources:
+            forward(d, last + i)
+        for d in sources:
+            if i > 0:
+                forwards[d, last + i - 1].wait_recv()
+                add_slice(d, 1, others[d], i - 1)
+            add_slice(d, 0, sources[d], i)
+            if i == final:
+                state = attend(state, sources[d], last, 1)
+    for d in sources:
+        forwards[d, last + final].wait_recv()
+        add_slice(d, 1, others[d], final)
+        state = attend(state, others[d], last, 1)
+
     highest, total, read = state
     head_of = lax.broadcasted_iota(jnp.int32, (MAP_ROWS, wide), 0) // 2
     own = jnp.zeros((MAP_ROWS, wide), jnp.float32)
@@ -209,26 +271,29 @@
         copy.wait_recv()
     heights = stats[:, 1]
     tops = heights[:, :, 0:1]
-    sums = heights[:, :, 1:2]
+    totals = heights[:, :, 1:2]
     factor = jnp.exp(tops - jnp.max(tops, axis=0, keepdims=True))
-    totals = jnp.sum(sums * factor, axis=0)
-    reads = jnp.sum(stats[:, 0] * factor, axis=0) / totals
-    normed = []
-    for h in range(heads):
-        diff = reads[2 * h:2 * h + 1] - lam[0:1, h:h + 1] * reads[2 * h + 1:2 * h + 2]
-        scale = lax.rsqrt(jnp.mean(diff * diff, axis=1, keepdims=True) + 1e-06)
-        normed.append(diff * scale * gain[...])
-    headed = jnp.concatenate(normed, axis=1)
-    headed = jnp.broadcast_to(headed, (MAP_ROWS, headed.shape[1])).astype(jnp.bfloat16)
-    partials = jnp.dot(headed, wo[...], preferred_element_type=jnp.float32).astype(jnp.bfloat16)
+    reads = jnp.sum(stats[:, 0] * factor, axis=0) / jnp.sum(totals * factor, axis=0)
+    diff = reads - lam_row * pltpu.roll(reads, maps - 1, 0)
+    scale = lax.rsqrt(jnp.mean(diff * diff, axis=1, keepdims=True) + 1e-06)
+    normed = diff * scale * gain[...]
+    headed = jnp.concatenate(
+        [
+            jnp.broadcast_to(normed[2 * h:2 * h + 1], (MAP_ROWS, wide)).astype(jnp.bfloat16)
+            for h in range(heads)
+        ],
+        axis=1,
+    )
+    partials = jnp.dot(headed, wo[...], preferred_element_type=jnp.float32)
+    partials = partials[:8].astype(jnp.bfloat16).astype(jnp.float32)
     for b in range(n_tp):
         part[b] = partials[:, b * out_cols:(b + 1) * out_cols]
     swaps = []
     for d in range(n_tp - 1, 0, -1):
         target = lax.rem(tp + d, n_tp)
         copy = pltpu.make_async_remote_copy(
-            src_ref=part.at[target],
-            dst_ref=parts.at[d - 1],
+            src_ref=part.at[target, pl.ds(0, 1)],
+            dst_ref=parts.at[d - 1, pl.ds(0, 1)],
             send_sem=pt_send.at[d - 1],
             recv_sem=pt_recv.at[d - 1],
             device_id={"tp": target},
@@ -236,16 +301,29 @@
         )
         copy.start()
         swaps.append(copy)
-    mixed = part[tp].astype(jnp.float32)
+    mixed = part[tp, 0:1]
     for copy in swaps:
         copy.wait_recv()
     for d in range(1, n_tp):
-        mixed = mixed + parts[d - 1].astype(jnp.float32)
-    mix_ref[...] = mixed[0:1].astype(jnp.bfloat16)
+        mixed = mixed + parts[d - 1, 0:1]
+    mix_ref[...] = mixed.astype(jnp.bfloat16)
 
     near.wait_send()
-    for copy in list(far.values()) + forwards + exchanges + swaps:
+    for copy in list(far.values()) + list(forwards.values()) + exchanges + swaps:
         copy.wait_send()
+
+
+def deliver(keys, values, mixed, key_out, value_out, mix_out, sem):
+    copies = [
+        pltpu.make_async_copy(source, target, sem.at[i])
+        for i, (source, target) in enumerate(
+            ((keys, key_out), (values, value_out), (mixed, mix_out))
+        )
+    ]
+    for copy in copies:
+        copy.start()
+    for copy in copies:
+        copy.wait()
 
 
 def tables(length, chunk, head_dim):
@@ -271,22 +349,25 @@
     chunk = rows // 4
     steps = rows // chunk
     chips = n_tp // 2
+    pieces = steps - 1 + len(SLICES)
     out_cols = out_weight.shape[1] // n_tp
     fine, coarse = tables(n_sp * n_tp * rows, chunk, head_dim)
     hbm_spec = pl.BlockSpec(memory_space=pltpu.HBM)
+    vmem_spec = pl.BlockSpec(memory_space=pltpu.VMEM)
     dma = pltpu.SemaphoreType.DMA
     bf16 = jnp.bfloat16
     f32 = jnp.float32
     room = 2 * n_tp * rows * columns * 2 + SMALL_BYTES
+    cache = (n_tp, rows, columns)
     k, v, mixed = pl.pallas_call(
         functools.partial(kernel, n_sp, n_tp, heads, head_dim, chunk),
         out_shape=(
-            pltpu.VMEM((n_tp, rows, columns), bf16),
-            pltpu.VMEM((n_tp, rows, columns), bf16),
-            jax.ShapeDtypeStruct((1, out_cols), bf16),
+            pltpu.VMEM(cache, bf16),
+            pltpu.VMEM(cache, bf16),
+            pltpu.VMEM((1, out_cols), bf16),
         ),
         in_specs=[hbm_spec] * 9,
-        out_specs=(pl.BlockSpec(memory_space=pltpu.VMEM),) * 3,
+        out_specs=(vmem_spec,) * 3,
         scratch_shapes=[
             pltpu.VMEM((n_tp, rows, depth), bf16),
             pltpu.VMEM((depth, columns), bf16),
@@ -298,17 +379,19 @@
             pltpu.VMEM((2, chunk, wide), f32),
             pltpu.VMEM((n_tp * steps, 2, wide), f32),
             pltpu.VMEM((n_sp, 2, 2 * heads, wide), f32),
-            pltpu.VMEM((n_tp, MAP_ROWS, out_cols), bf16),
-            pltpu.VMEM((n_tp - 1, MAP_ROWS, out_cols), bf16),
+            pltpu.VMEM((n_tp, 8, out_cols), f32),
+            pltpu.VMEM((n_tp - 1, 8, out_cols), f32),
+            pltpu.VMEM((2 * (chips - 1), chunk, 2 * columns), f32),
             dma((9,)),
+            dma((steps,)),
             pltpu.SemaphoreType.REGULAR,
             pltpu.SemaphoreType.REGULAR,
             dma,
             dma,
-            dma((chips - 1, steps)),
-            dma((chips - 1, steps)),
-            dma((chips - 1, steps)),
-            dma((chips - 1, steps)),
+            dma((chips - 1, pieces)),
+            dma((chips - 1, pieces)),
+            dma((chips - 1, pieces)),
+            dma((chips - 1, pieces)),
             dma((n_sp - 1,)),
             dma((n_sp - 1,)),
             dma((n_tp - 1,)),
@@ -321,6 +404,18 @@
         x, key_weight, value_weight, new_queries, lambdas.reshape(1, heads),
         head_gain.reshape(1, wide), out_weight, jnp.asarray(fine), jnp.asarray(coarse),
     )
+    k, v, mixed = pl.pallas_call(
+        deliver,
+        out_shape=(
+            jax.ShapeDtypeStruct(cache, bf16),
+            jax.ShapeDtypeStruct(cache, bf16),
+            jax.ShapeDtypeStruct((1, out_cols), bf16),
+        ),
+        in_specs=[vmem_spec] * 3,
+        out_specs=(hbm_spec,) * 3,
+        scratch_shapes=[dma((3,))],
+        compiler_params=pltpu.CompilerParams(vmem_limit_bytes=2**20),
+    )(k, v, mixed)
     full = (1, n_tp * rows, columns)
     return k.reshape(full), v.reshape(full), mixed
 

time: 37 us -> 35.4 us (0.957)
  local copies, waits for them, and re-layouts: 2.34 us -> 0 us
  Pallas kernels: 33.9 us -> 34.5 us
    unnamed x5 -> x0, local copies, waits for them, and re-layouts: 2.34 us -> none
    pallas_call x0 -> x1, Pallas kernels: none -> 1.17 us  [on_device(): pl.pallas_call(deliver, out_shape=(jax.ShapeDtypeStruct(cache, bf16), jax...]
    pallas_call x1, Pallas kernels: 33.9 us -> 33.4 us  [on_device(): pl.pallas_call(functools.partial(kernel, n_sp, n_tp, heads, head_dim, chu...]
where the time goes in v1:
time: 35.4 us; the launch traced here: 35.2 us
  Pallas kernels  34.5 us (97%)
  between operations  0.64 us (2%)
    pallas_call x1, Pallas kernels, on_device(): pl.pallas_call(functools.partial(kernel, n_sp, n_tp, heads, head_dim, chu...  33.4 us
    pallas_call x1, Pallas kernels, on_device(): pl.pallas_call(deliver, out_shape=(jax.ShapeDtypeStruct(cache, bf16), jax...  1.17 us

profile of v1, /device:TPU:0, one launch (start us, length us, event | category | flops | bytes accessed | tf_op | source)
XLA Modules:
  0.0 35.2 jit_solution(11751644150683513146)
XLA Ops:
  0.6 33.4 %shard_map.112 = (bf16[4,192,512]{2,1,0:T(8,128)(2,1)S(1)}, bf16[4,192,512]{2,1,0:T(8,128)(2,1)S(1)}, bf16[1,512]{1,0:T(2,128)(2,1)S(1)}) custom-call(bf16[1,192,2048]{2,1,0:T(8,128)(2,1)} %x_ref.1, bf16[2048,512]{1,0:T(8,128)(2,1)} %wk_ref.1, bf16[2048,512]{1,0:T(8,128)(2,1)} %wv_ref.1, bf16[1,512]{1,0:T(2,128)(2,1)} %q_ref.1, f32[1,4]{1,0:T(1,128)} %bitcast.4, ...), custom_call_target="tpu_custom_call" | custom-call | tf_op jit(solution)/shard_map/pallas_call | solution.py:362
  34.0 1.2 %shard_map.113 = (bf16[4,192,512]{2,1,0:T(8,128)(2,1)}, bf16[4,192,512]{2,1,0:T(8,128)(2,1)}, bf16[1,512]{1,0:T(2,128)(2,1)}) custom-call(bf16[4,192,512]{2,1,0:T(8,128)(2,1)S(1)} %get-tuple-element.9.keys, bf16[4,192,512]{2,1,0:T(8,128)(2,1)S(1)} %get-tuple-element.10.values, bf16[1,512]{1,0:T(2,128)(2,1)S(1)} %get-tuple-element.11.mixed), custom_call_target="tpu_custom_call" | custom-call | tf_op jit(solution)/shard_map/pallas_call | solution.py:407

commit v2 on v1

--- a/solution.py
+++ b/solution.py
@@ -93,7 +93,7 @@
                 dst_ref=piece_of(tp, p),
                 send_sem=far_send.at[d - 1, p],
                 recv_sem=far_recv.at[d - 1, p],
-                device_id={"tp": lax.rem(tp + 2 * d, n_tp)},
+                device_id={"tp": lax.rem(partner + 2 * d, n_tp)},
                 device_id_type=MESH,
             )
             far[d, p].start()
@@ -193,7 +193,7 @@
     for h in range(heads):
         lam_row = jnp.where(map_of == 2 * h, lam[0:1, h:h + 1], lam_row)
 
-    sources = {d: lax.rem(tp + n_tp - 2 * d, n_tp) for d in range(1, chips)}
+    sources = {d: lax.rem(partner + n_tp - 2 * d, n_tp) for d in range(1, chips)}
     others = {d: sources[d] + 1 - 2 * lax.rem(sources[d], 2) for d in sources}
     forwards = {}
 
@@ -234,13 +234,15 @@
     for i in range(len(cuts)):
         for d in sources:
             forward(d, last + i)
-        for d in sources:
-            if i > 0:
-                forwards[d, last + i - 1].wait_recv()
-                add_slice(d, 1, others[d], i - 1)
+            if i > 1:
+                forwards[d, last + i - 2].wait_recv()
             add_slice(d, 0, sources[d], i)
-            if i == final:
-                state = attend(state, sources[d], last, 1)
+            if i > 1:
+                add_slice(d, 1, others[d], i - 2)
+    for d in sources:
+        forwards[d, last + final - 1].wait_recv()
+        state = attend(state, sources[d], last, 1)
+        add_slice(d, 1, others[d], final - 1)
     for d in sources:
         forwards[d, last + final].wait_recv()
         add_slice(d, 1, others[d], final)

time: 35.4 us -> 34.5 us (0.975)
  Pallas kernels: 34.5 us -> 33.7 us
    pallas_call x1, Pallas kernels: 33.4 us -> 32.5 us  [on_device(): pl.pallas_call(functools.partial(kernel, n_sp, n_tp, heads, head_dim, chu...]
where the time goes in v2:
time: 34.5 us; the launch traced here: 34.3 us
  Pallas kernels  33.7 us (98%)
  between operations  0.64 us (2%)
    pallas_call x1, Pallas kernels, on_device(): pl.pallas_call(functools.partial(kernel, n_sp, n_tp, heads, head_dim, chu...  32.5 us
    pallas_call x1, Pallas kernels, on_device(): pl.pallas_call(deliver, out_shape=(jax.ShapeDtypeStruct(cache, bf16), jax...  1.17 us

profile of v2, /device:TPU:0, one launch (start us, length us, event | category | flops | bytes accessed | tf_op | source)
XLA Modules:
  0.0 34.3 jit_solution(5947046134875460237)
XLA Ops:
  0.6 32.5 %shard_map.112 = (bf16[4,192,512]{2,1,0:T(8,128)(2,1)S(1)}, bf16[4,192,512]{2,1,0:T(8,128)(2,1)S(1)}, bf16[1,512]{1,0:T(2,128)(2,1)S(1)}) custom-call(bf16[1,192,2048]{2,1,0:T(8,128)(2,1)} %x_ref.1, bf16[2048,512]{1,0:T(8,128)(2,1)} %wk_ref.1, bf16[2048,512]{1,0:T(8,128)(2,1)} %wv_ref.1, bf16[1,512]{1,0:T(2,128)(2,1)} %q_ref.1, f32[1,4]{1,0:T(1,128)} %bitcast.4, ...), custom_call_target="tpu_custom_call" | custom-call | tf_op jit(solution)/shard_map/pallas_call | solution.py:364
  33.1 1.2 %shard_map.113 = (bf16[4,192,512]{2,1,0:T(8,128)(2,1)}, bf16[4,192,512]{2,1,0:T(8,128)(2,1)}, bf16[1,512]{1,0:T(2,128)(2,1)}) custom-call(bf16[4,192,512]{2,1,0:T(8,128)(2,1)S(1)} %get-tuple-element.9.keys, bf16[4,192,512]{2,1,0:T(8,128)(2,1)S(1)} %get-tuple-element.10.values, bf16[1,512]{1,0:T(2,128)(2,1)S(1)} %get-tuple-element.11.mixed), custom_call_target="tpu_custom_call" | custom-call | tf_op jit(solution)/shard_map/pallas_call | solution.py:409

commit v3 on v2

--- a/solution.py
+++ b/solution.py
@@ -21,7 +21,7 @@
     keys, values, mix_ref,
     xg, wk, wv, wo, q, lam, gain, fine, coarse, stats, part, parts, sums,
     load_sem, own_sem, up_sem, down_sem, near_send, near_recv, far_send, far_recv, fwd_send, fwd_recv,
-    st_send, st_recv, pt_send, pt_recv,
+    wo_send, wo_recv, st_send, st_recv, pt_send, pt_recv,
 ):
     sp = lax.axis_index("sp")
     tp = lax.axis_index("tp")
@@ -31,7 +31,9 @@
     maps = 2 * heads
     steps = rows // chunk
     chips = n_tp // 2
-    partner = tp + 1 - 2 * lax.rem(tp, 2)
+    core = lax.rem(tp, 2)
+    partner = tp + 1 - 2 * core
+    is_lead = core == 1
     out_cols = mix_ref.shape[1]
     local_coarse = n_tp * steps
     last = steps - 1
@@ -60,8 +62,16 @@
         ),
         pltpu.make_async_copy(lam_ref, lam, load_sem.at[6]),
         pltpu.make_async_copy(gain_ref, gain, load_sem.at[7]),
-        pltpu.make_async_copy(wo_ref, wo, load_sem.at[8]),
     ]
+    own_wo = pltpu.make_async_copy(wo_ref, wo.at[pl.ds(columns, columns)], load_sem.at[8])
+    lent_wo = pltpu.make_async_remote_copy(
+        src_ref=wo_ref,
+        dst_ref=wo.at[pl.ds(0, columns)],
+        send_sem=wo_send,
+        recv_sem=wo_recv,
+        device_id={"tp": partner},
+        device_id_type=MESH,
+    )
 
     barrier = pltpu.get_barrier_semaphore()
     for d in range(1, n_tp):
@@ -108,6 +118,8 @@
     near.start()
     for load in loads:
         load.start()
+    pl.when(is_lead)(own_wo.start)
+    pl.when(core == 0)(lent_wo.start)
 
     lane = lax.broadcasted_iota(jnp.int32, (chunk, wide), 1)
     low_half = lax.rem(lane, head_dim) < head_dim // 2
@@ -253,65 +265,104 @@
     own = jnp.zeros((MAP_ROWS, wide), jnp.float32)
     for h in range(heads):
         own = jnp.where(head_of == h, read[:, h * wide:(h + 1) * wide], own)
-    first_lane = lax.broadcasted_iota(jnp.int32, (MAP_ROWS, wide), 1) == 0
-    stats[sp, 0] = own[:maps]
-    stats[sp, 1] = jnp.where(first_lane, highest, total)[:maps]
-
-    exchanges = []
-    for d in range(n_sp - 1, 0, -1):
-        copy = pltpu.make_async_remote_copy(
-            src_ref=stats.at[sp],
-            dst_ref=stats.at[sp],
-            send_sem=st_send.at[d - 1],
-            recv_sem=st_recv.at[d - 1],
-            device_id={"sp": lax.rem(sp + d, n_sp)},
+    lane_of = lax.broadcasted_iota(jnp.int32, (maps, wide), 1)
+    stats[sp, core, 0] = own[:maps]
+    stats[sp, core, 1] = jnp.where(
+        lane_of == 0, highest[:maps], jnp.where(lane_of == 1, total[:maps], lam_row)
+    )
+
+    def stats_copy(d):
+        return pltpu.make_async_remote_copy(
+            src_ref=stats.at[sp, core],
+            dst_ref=stats.at[sp, core],
+            send_sem=st_send.at[d],
+            recv_sem=st_recv.at[d, core],
+            device_id={"sp": lax.rem(sp + d, n_sp), "tp": tp + 1 - core},
             device_id_type=MESH,
         )
+
+    def stats_arrival(d, source):
+        return pltpu.make_async_remote_copy(
+            src_ref=stats.at[sp, source],
+            dst_ref=stats.at[sp, source],
+            send_sem=st_send.at[d],
+            recv_sem=st_recv.at[d, source],
+            device_id={"tp": partner},
+            device_id_type=MESH,
+        )
+
+    exchanges = [stats_copy(d) for d in range(n_sp - 1, 0, -1)]
+    for copy in exchanges:
         copy.start()
-        exchanges.append(copy)
-    for copy in exchanges:
-        copy.wait_recv()
-    heights = stats[:, 1]
-    tops = heights[:, :, 0:1]
-    totals = heights[:, :, 1:2]
-    factor = jnp.exp(tops - jnp.max(tops, axis=0, keepdims=True))
-    reads = jnp.sum(stats[:, 0] * factor, axis=0) / jnp.sum(totals * factor, axis=0)
-    diff = reads - lam_row * pltpu.roll(reads, maps - 1, 0)
-    scale = lax.rsqrt(jnp.mean(diff * diff, axis=1, keepdims=True) + 1e-06)
-    normed = diff * scale * gain[...]
-    headed = jnp.concatenate(
-        [
-            jnp.broadcast_to(normed[2 * h:2 * h + 1], (MAP_ROWS, wide)).astype(jnp.bfloat16)
-            for h in range(heads)
-        ],
-        axis=1,
-    )
-    partials = jnp.dot(headed, wo[...], preferred_element_type=jnp.float32)
-    partials = partials[:8].astype(jnp.bfloat16).astype(jnp.float32)
-    for b in range(n_tp):
-        part[b] = partials[:, b * out_cols:(b + 1) * out_cols]
-    swaps = []
-    for d in range(n_tp - 1, 0, -1):
-        target = lax.rem(tp + d, n_tp)
-        copy = pltpu.make_async_remote_copy(
-            src_ref=part.at[target, pl.ds(0, 1)],
-            dst_ref=parts.at[d - 1, pl.ds(0, 1)],
-            send_sem=pt_send.at[d - 1],
-            recv_sem=pt_recv.at[d - 1],
-            device_id={"tp": target},
+    pl.when(core == 0)(stats_copy(0).start)
+
+    def share_copy(d, target):
+        chip = lax.rem(tp // 2 + d, chips)
+        return pltpu.make_async_remote_copy(
+            src_ref=part.at[d, target, pl.ds(0, 1)],
+            dst_ref=parts.at[d, pl.ds(0, 1)],
+            send_sem=pt_send.at[d, target],
+            recv_sem=pt_recv.at[d],
+            device_id={"tp": 2 * chip + target},
             device_id_type=MESH,
         )
-        copy.start()
-        swaps.append(copy)
-    mixed = part[tp, 0:1]
-    for copy in swaps:
-        copy.wait_recv()
-    for d in range(1, n_tp):
-        mixed = mixed + parts[d - 1, 0:1]
-    mix_ref[...] = mixed.astype(jnp.bfloat16)
+
+    @pl.when(is_lead)
+    def _():
+        own_wo.wait()
+        lent_wo.wait_recv()
+        stats_arrival(0, 0).wait_recv()
+        for d in range(1, n_sp):
+            for source in range(2):
+                stats_arrival(d, source).wait_recv()
+        headed = []
+        for c in range(2):
+            heights = stats[:, c, 1]
+            tops = heights[:, :, 0:1]
+            totals = heights[:, :, 1:2]
+            factor = jnp.exp(tops - jnp.max(tops, axis=0, keepdims=True))
+            reads = jnp.sum(stats[:, c, 0] * factor, axis=0) / jnp.sum(totals * factor, axis=0)
+            diff = reads - heights[0, :, 2:3] * pltpu.roll(reads, maps - 1, 0)
+            scale = lax.rsqrt(jnp.mean(diff * diff, axis=1, keepdims=True) + 1e-06)
+            normed = diff * scale * gain[...]
+            row_of = lax.broadcasted_iota(jnp.int32, (MAP_ROWS, wide), 0)
+            headed += [
+                jnp.where(row_of == c, normed[2 * h:2 * h + 1], 0.0).astype(jnp.bfloat16)
+                for h in range(heads)
+            ]
+        headed = jnp.concatenate(headed, axis=1)
+        for d in list(range(1, chips)) + [0]:
+            first = pl.multiple_of(lax.rem(tp // 2 + d, chips) * 2 * out_cols, 2 * out_cols)
+            partials = jnp.dot(
+                headed, wo[:, pl.ds(first, 2 * out_cols)], preferred_element_type=jnp.float32
+            )[:8].astype(jnp.bfloat16).astype(jnp.float32)
+            both = partials + pltpu.roll(partials, 7, 0)
+            for target in range(2):
+                part[d, target] = both[:, target * out_cols:(target + 1) * out_cols]
+                if d > 0 or target == 0:
+                    share_copy(d, target).start()
+        mixed = part[0, 1, 0:1]
+        for d in range(1, chips):
+            share_copy(d, 1).wait_recv()
+            mixed = mixed + parts[d, 0:1]
+        mix_ref[...] = mixed.astype(jnp.bfloat16)
+        for d in range(chips):
+            for target in range(2):
+                if d > 0 or target == 0:
+                    share_copy(d, target).wait_send()
+
+    @pl.when(core == 0)
+    def _():
+        mixed = None
+        for d in range(chips):
+            share_copy(d, 1).wait_recv()
+            mixed = parts[d, 0:1] if mixed is None else mixed + parts[d, 0:1]
+        mix_ref[...] = mixed.astype(jnp.bfloat16)
+        lent_wo.wait_send()
+        stats_copy(0).wait_send()
 
     near.wait_send()
-    for copy in list(far.values()) + list(forwards.values()) + exchanges + swaps:
+    for copy in list(far.values()) + list(forwards.values()) + exchanges:
         copy.wait_send()
 
 
@@ -374,15 +425,15 @@
             pltpu.VMEM((n_tp, rows, depth), bf16),
             pltpu.VMEM((depth, columns), bf16),
             pltpu.VMEM((depth, columns), bf16),
-            pltpu.VMEM(out_weight.shape, bf16),
+            pltpu.VMEM((2 * columns, out_weight.shape[1]), bf16),
             pltpu.VMEM((1, columns), bf16),
             pltpu.VMEM((1, heads), f32),
             pltpu.VMEM((1, wide), f32),
             pltpu.VMEM((2, chunk, wide), f32),
             pltpu.VMEM((n_tp * steps, 2, wide), f32),
-            pltpu.VMEM((n_sp, 2, 2 * heads, wide), f32),
-            pltpu.VMEM((n_tp, 8, out_cols), f32),
-            pltpu.VMEM((n_tp - 1, 8, out_cols), f32),
+            pltpu.VMEM((n_sp, 2, 2, 2 * heads, wide), f32),
+            pltpu.VMEM((chips, 2, 8, out_cols), f32),
+            pltpu.VMEM((chips, 8, out_cols), f32),
             pltpu.VMEM((2 * (chips - 1), chunk, 2 * columns), f32),
             dma((9,)),
             dma((steps,)),
@@ -394,10 +445,12 @@
             dma((chips - 1, pieces)),
             dma((chips - 1, pieces)),
             dma((chips - 1, pieces)),
-            dma((n_sp - 1,)),
-            dma((n_sp - 1,)),
-            dma((n_tp - 1,)),
-            dma((n_tp - 1,)),
+            dma,
+            dma,
+            dma((n_sp,)),
+            dma((n_sp, 2)),
+            dma((chips, 2)),
+            dma((chips,)),
         ],
         compiler_params=pltpu.CompilerParams(
             collective_id=0, has_side_effects=True, vmem_limit_bytes=VMEM_BYTES - room

time: 34.5 us -> 33.6 us (0.974)
  Pallas kernels: 33.7 us -> 32.7 us
    pallas_call x1, Pallas kernels: 32.5 us -> 31.6 us  [on_device(): pl.pallas_call(functools.partial(kernel, n_sp, n_tp, heads, head_dim, chu...]
where the time goes in v3:
time: 33.6 us; the launch traced here: 33.4 us
  Pallas kernels  32.7 us (97%)
  between operations  0.64 us (2%)
    pallas_call x1, Pallas kernels, on_device(): pl.pallas_call(functools.partial(kernel, n_sp, n_tp, heads, head_dim, chu...  31.6 us
    pallas_call x1, Pallas kernels, on_device(): pl.pallas_call(deliver, out_shape=(jax.ShapeDtypeStruct(cache, bf16), jax...  1.17 us

profile of v3, /device:TPU:0, one launch (start us, length us, event | category | flops | bytes accessed | tf_op | source)
XLA Modules:
  0.0 33.4 jit_solution(16654559447249549373)
XLA Ops:
  0.6 31.6 %shard_map.112 = (bf16[4,192,512]{2,1,0:T(8,128)(2,1)S(1)}, bf16[4,192,512]{2,1,0:T(8,128)(2,1)S(1)}, bf16[1,512]{1,0:T(2,128)(2,1)S(1)}) custom-call(bf16[1,192,2048]{2,1,0:T(8,128)(2,1)} %x_ref.1, bf16[2048,512]{1,0:T(8,128)(2,1)} %wk_ref.1, bf16[2048,512]{1,0:T(8,128)(2,1)} %wv_ref.1, bf16[1,512]{1,0:T(2,128)(2,1)} %q_ref.1, f32[1,4]{1,0:T(1,128)} %bitcast.4, ...), custom_call_target="tpu_custom_call" | custom-call | tf_op jit(solution)/shard_map/pallas_call | solution.py:415
  32.2 1.2 %shard_map.113 = (bf16[4,192,512]{2,1,0:T(8,128)(2,1)}, bf16[4,192,512]{2,1,0:T(8,128)(2,1)}, bf16[1,512]{1,0:T(2,128)(2,1)}) custom-call(bf16[4,192,512]{2,1,0:T(8,128)(2,1)S(1)} %get-tuple-element.9.keys, bf16[4,192,512]{2,1,0:T(8,128)(2,1)S(1)} %get-tuple-element.10.values, bf16[1,512]{1,0:T(2,128)(2,1)S(1)} %get-tuple-element.11.mixed), custom_call_target="tpu_custom_call" | custom-call | tf_op jit(solution)/shard_map/pallas_call | solution.py:462

commit v4 on v3

--- a/solution.py
+++ b/solution.py
@@ -20,7 +20,8 @@
     x_ref, wk_ref, wv_ref, q_ref, lam_ref, gain_ref, wo_ref, fine_ref, coarse_ref,
     keys, values, mix_ref,
     xg, wk, wv, wo, q, lam, gain, fine, coarse, stats, part, parts, sums,
-    load_sem, own_sem, up_sem, down_sem, near_send, near_recv, far_send, far_recv, fwd_send, fwd_recv,
+    load_sem, own_sem, up_sem, down_sem, near_send, near_recv, far_send, far_recv, twin_send, twin_recv,
+    fwd_send, fwd_recv,
     wo_send, wo_recv, st_send, st_recv, pt_send, pt_recv,
 ):
     sp = lax.axis_index("sp")
@@ -94,7 +95,7 @@
     pl.semaphore_wait(barrier, n_tp - 1 + jnp.where(has_lower, 1, 0) + jnp.where(has_upper, 1, 0))
 
     far = {}
-    for p in range(len(pieces)):
+    for p in range(len(pieces) - 1):
         if p < steps:
             own_loads[p].wait()
         for d in range(1, chips):
@@ -107,6 +108,18 @@
                 device_id_type=MESH,
             )
             far[d, p].start()
+    twins = {}
+    for d in range(1, chips):
+        for target in range(2):
+            twins[d, target] = pltpu.make_async_remote_copy(
+                src_ref=piece_of(tp, len(pieces) - 1),
+                dst_ref=piece_of(tp, len(pieces) - 1),
+                send_sem=twin_send.at[d - 1, target],
+                recv_sem=twin_recv.at[d - 1, core],
+                device_id={"tp": lax.rem(tp - core + 2 * d, n_tp) + target},
+                device_id_type=MESH,
+            )
+            twins[d, target].start()
     near = pltpu.make_async_remote_copy(
         src_ref=xg.at[tp],
         dst_ref=xg.at[tp],
@@ -155,24 +168,31 @@
     map_col = lax.broadcasted_iota(jnp.int32, (MAP_ROWS, columns), 1) // head_dim
     spread = jnp.where(map_row == map_col, q[...].astype(jnp.float32), 0.0).astype(jnp.bfloat16)
 
-    def attend(state, block, first, count):
+    def attend(state, blocks, first, count):
         where = slice(first * chunk, (first + count) * chunk)
-        score = lax.dot_general(
-            spread, keys[block, where, :], (((1,), (1,)), ((), ())),
-            preferred_element_type=jnp.float32,
-        ) * head_dim ** (-0.5)
-        highest = jnp.max(score, axis=1, keepdims=True)
+        scores = [
+            lax.dot_general(
+                spread, keys[block, where, :], (((1,), (1,)), ((), ())),
+                preferred_element_type=jnp.float32,
+            ) * head_dim ** (-0.5)
+            for block in blocks
+        ]
+        highest = functools.reduce(
+            jnp.maximum, [jnp.max(score, axis=1, keepdims=True) for score in scores]
+        )
         if state is not None:
             highest = jnp.maximum(highest, state[0])
-        weight = jnp.exp(score - highest)
-        total = jnp.sum(weight, axis=1, keepdims=True)
-        upper = weight.astype(jnp.bfloat16)
-        lower = (weight - upper.astype(jnp.float32)).astype(jnp.bfloat16)
-        read = jnp.dot(
-            jnp.concatenate([upper, lower], axis=0), values[block, where, :],
-            preferred_element_type=jnp.float32,
-        )
-        read = read[:MAP_ROWS] + read[MAP_ROWS:]
+        total, read = 0.0, 0.0
+        for block, score in zip(blocks, scores):
+            weight = jnp.exp(score - highest)
+            total = total + jnp.sum(weight, axis=1, keepdims=True)
+            upper = weight.astype(jnp.bfloat16)
+            lower = (weight - upper.astype(jnp.float32)).astype(jnp.bfloat16)
+            both = jnp.dot(
+                jnp.concatenate([upper, lower], axis=0), values[block, where, :],
+                preferred_element_type=jnp.float32,
+            )
+            read = read + both[:MAP_ROWS] + both[MAP_ROWS:]
         if state is not None:
             fade = jnp.exp(state[0] - highest)
             total = total + state[1] * fade
@@ -180,7 +200,7 @@
         return highest, total, read
 
     project(tp, 0, steps)
-    state = attend(None, tp, 0, steps)
+    state = attend(None, [tp], 0, steps)
 
     pl.when(has_lower)(lambda: pl.semaphore_wait(up_sem, 1))
 
@@ -190,7 +210,7 @@
 
     near.wait_recv()
     project(partner, 0, steps)
-    state = attend(state, partner, 0, steps)
+    state = attend(state, [partner], 0, steps)
 
     pl.when(has_upper)(lambda: pl.semaphore_wait(down_sem, 1))
 
@@ -225,10 +245,10 @@
         for d in sources:
             forward(d, j)
             project(sources[d], j, 1)
-            state = attend(state, sources[d], j, 1)
+            state = attend(state, [sources[d]], j, 1)
             forwards[d, j].wait_recv()
             project(others[d], j, 1)
-            state = attend(state, others[d], j, 1)
+            state = attend(state, [others[d]], j, 1)
 
     def add_slice(d, side, block, i):
         raw_keys, raw_values = product(block, last, 1, cuts[i])
@@ -236,14 +256,11 @@
         if i > 0:
             raw_keys = raw_keys + sums[slot, :, :columns]
             raw_values = raw_values + sums[slot, :, columns:]
-        if i < len(cuts) - 1:
-            sums[slot, :, :columns] = raw_keys
-            sums[slot, :, columns:] = raw_values
-        else:
-            settle(block, last, 1, raw_keys, raw_values)
+        sums[slot, :, :columns] = raw_keys
+        sums[slot, :, columns:] = raw_values
 
     final = len(cuts) - 1
-    for i in range(len(cuts)):
+    for i in range(final):
         for d in sources:
             forward(d, last + i)
             if i > 1:
@@ -251,14 +268,35 @@
             add_slice(d, 0, sources[d], i)
             if i > 1:
                 add_slice(d, 1, others[d], i - 2)
+    for i in range(max(final - 2, 0), final):
+        for d in sources:
+            forwards[d, last + i].wait_recv()
+            add_slice(d, 1, others[d], i)
     for d in sources:
-        forwards[d, last + final - 1].wait_recv()
-        state = attend(state, sources[d], last, 1)
-        add_slice(d, 1, others[d], final - 1)
-    for d in sources:
-        forwards[d, last + final].wait_recv()
-        add_slice(d, 1, others[d], final)
-        state = attend(state, others[d], last, 1)
+        pair = (sources[d], others[d])
+        for source in range(2):
+            pltpu.make_async_remote_copy(
+                src_ref=piece_of(sources[d], len(pieces) - 1),
+                dst_ref=piece_of(sources[d], len(pieces) - 1),
+                send_sem=twin_send.at[d - 1, source],
+                recv_sem=twin_recv.at[d - 1, source],
+                device_id={"tp": partner},
+                device_id_type=MESH,
+            ).wait_recv()
+        piece = jnp.concatenate(
+            [xg[block, last * chunk:rows, cuts[final]] for block in pair], axis=0
+        )
+        raw_keys = jnp.dot(piece, wk[cuts[final], :], preferred_element_type=jnp.float32)
+        raw_values = jnp.dot(piece, wv[cuts[final], :], preferred_element_type=jnp.float32)
+        for side, block in enumerate(pair):
+            slot = 2 * (d - 1) + side
+            part_of = slice(side * chunk, (side + 1) * chunk)
+            settle(
+                block, last, 1,
+                raw_keys[part_of] + sums[slot, :, :columns],
+                raw_values[part_of] + sums[slot, :, columns:],
+            )
+        state = attend(state, pair, last, 1)
 
     highest, total, read = state
     head_of = lax.broadcasted_iota(jnp.int32, (MAP_ROWS, wide), 0) // 2
@@ -271,13 +309,14 @@
         lane_of == 0, highest[:maps], jnp.where(lane_of == 1, total[:maps], lam_row)
     )
 
-    def stats_copy(d):
+    def stats_copy(target):
+        d = lax.rem(target + n_sp - sp, n_sp)
         return pltpu.make_async_remote_copy(
             src_ref=stats.at[sp, core],
             dst_ref=stats.at[sp, core],
             send_sem=st_send.at[d],
             recv_sem=st_recv.at[d, core],
-            device_id={"sp": lax.rem(sp + d, n_sp), "tp": tp + 1 - core},
+            device_id={"sp": target, "tp": tp + 1 - core},
             device_id_type=MESH,
         )
 
@@ -291,10 +330,12 @@
             device_id_type=MESH,
         )
 
-    exchanges = [stats_copy(d) for d in range(n_sp - 1, 0, -1)]
-    for copy in exchanges:
-        copy.start()
-    pl.when(core == 0)(stats_copy(0).start)
+    exchanges = []
+    for k in range(n_sp - 1):
+        up, down = k + jnp.where(k >= sp, 1, 0), n_sp - 1 - k - jnp.where(n_sp - 1 - k <= sp, 1, 0)
+        exchanges.append(stats_copy(jnp.where(2 * sp >= n_sp, up, down)))
+        exchanges[-1].start()
+    pl.when(core == 0)(stats_copy(sp).start)
 
     def share_copy(d, target):
         chip = lax.rem(tp // 2 + d, chips)
@@ -315,7 +356,8 @@
         for d in range(1, n_sp):
             for source in range(2):
                 stats_arrival(d, source).wait_recv()
-        headed = []
+        headed, scales = [], []
+        row_of = lax.broadcasted_iota(jnp.int32, (2 * MAP_ROWS, wide), 0)
         for c in range(2):
             heights = stats[:, c, 1]
             tops = heights[:, :, 0:1]
@@ -323,22 +365,30 @@
             factor = jnp.exp(tops - jnp.max(tops, axis=0, keepdims=True))
             reads = jnp.sum(stats[:, c, 0] * factor, axis=0) / jnp.sum(totals * factor, axis=0)
             diff = reads - heights[0, :, 2:3] * pltpu.roll(reads, maps - 1, 0)
-            scale = lax.rsqrt(jnp.mean(diff * diff, axis=1, keepdims=True) + 1e-06)
-            normed = diff * scale * gain[...]
-            row_of = lax.broadcasted_iota(jnp.int32, (MAP_ROWS, wide), 0)
+            scales.append(lax.rsqrt(jnp.mean(diff * diff, axis=1, keepdims=True) + 1e-06))
+            gained = diff * gain[...]
             headed += [
-                jnp.where(row_of == c, normed[2 * h:2 * h + 1], 0.0).astype(jnp.bfloat16)
+                jnp.where(
+                    row_of == c * MAP_ROWS + h, gained[2 * h:2 * h + 1], 0.0
+                ).astype(jnp.bfloat16)
                 for h in range(heads)
             ]
         headed = jnp.concatenate(headed, axis=1)
         for d in list(range(1, chips)) + [0]:
-            first = pl.multiple_of(lax.rem(tp // 2 + d, chips) * 2 * out_cols, 2 * out_cols)
-            partials = jnp.dot(
-                headed, wo[:, pl.ds(first, 2 * out_cols)], preferred_element_type=jnp.float32
-            )[:8].astype(jnp.bfloat16).astype(jnp.float32)
-            both = partials + pltpu.roll(partials, 7, 0)
             for target in range(2):
-                part[d, target] = both[:, target * out_cols:(target + 1) * out_cols]
+                column = (2 * lax.rem(tp // 2 + d, chips) + target) * out_cols
+                first = pl.multiple_of(column, out_cols)
+                shares = jnp.dot(
+                    headed, wo[:, pl.ds(first, out_cols)], preferred_element_type=jnp.float32
+                )
+                both = 0.0
+                for c in range(2):
+                    group = 0.0
+                    for h in range(heads):
+                        row = c * MAP_ROWS + h
+                        group = group + shares[row:row + 1] * scales[c][2 * h:2 * h + 1]
+                    both = both + group.astype(jnp.bfloat16).astype(jnp.float32)
+                part[d, target, 0:1] = both
                 if d > 0 or target == 0:
                     share_copy(d, target).start()
         mixed = part[0, 1, 0:1]
@@ -359,10 +409,10 @@
             mixed = parts[d, 0:1] if mixed is None else mixed + parts[d, 0:1]
         mix_ref[...] = mixed.astype(jnp.bfloat16)
         lent_wo.wait_send()
-        stats_copy(0).wait_send()
+        stats_copy(sp).wait_send()
 
     near.wait_send()
-    for copy in list(far.values()) + list(forwards.values()) + exchanges:
+    for copy in [*far.values(), *twins.values(), *forwards.values(), *exchanges]:
         copy.wait_send()
 
 
@@ -441,10 +491,12 @@
             pltpu.SemaphoreType.REGULAR,
             dma,
             dma,
-            dma((chips - 1, pieces)),
-            dma((chips - 1, pieces)),
-            dma((chips - 1, pieces)),
-            dma((chips - 1, pieces)),
+            dma((chips - 1, pieces - 1)),
+            dma((chips - 1, pieces - 1)),
+            dma((chips - 1, 2)),
+            dma((chips - 1, 2)),
+            dma((chips - 1, pieces - 1)),
+            dma((chips - 1, pieces - 1)),
             dma,
             dma,
             dma((n_sp,)),

time: 33.6 us -> 33.3 us (level)
  no operation moved by 1% of the time
where the time goes in v4:
time: 33.3 us; the launch traced here: 33.1 us
  Pallas kernels  32.5 us (98%)
  between operations  0.64 us (2%)
    pallas_call x1, Pallas kernels, on_device(): pl.pallas_call(functools.partial(kernel, n_sp, n_tp, heads, head_dim, chu...  31.3 us
    pallas_call x1, Pallas kernels, on_device(): pl.pallas_call(deliver, out_shape=(jax.ShapeDtypeStruct(cache, bf16), jax...  1.17 us

profile of v4, /device:TPU:0, one launch (start us, length us, event | category | flops | bytes accessed | tf_op | source)
XLA Modules:
  0.0 33.1 jit_solution(8460302127174121605)
XLA Ops:
  0.6 31.3 %shard_map.112 = (bf16[4,192,512]{2,1,0:T(8,128)(2,1)S(1)}, bf16[4,192,512]{2,1,0:T(8,128)(2,1)S(1)}, bf16[1,512]{1,0:T(2,128)(2,1)S(1)}) custom-call(bf16[1,192,2048]{2,1,0:T(8,128)(2,1)} %x_ref.1, bf16[2048,512]{1,0:T(8,128)(2,1)} %wk_ref.1, bf16[2048,512]{1,0:T(8,128)(2,1)} %wv_ref.1, bf16[1,512]{1,0:T(2,128)(2,1)} %q_ref.1, f32[1,4]{1,0:T(1,128)} %bitcast.4, ...), custom_call_target="tpu_custom_call" | custom-call | tf_op jit(solution)/shard_map/pallas_call | solution.py:465
  31.9 1.2 %shard_map.113 = (bf16[4,192,512]{2,1,0:T(8,128)(2,1)}, bf16[4,192,512]{2,1,0:T(8,128)(2,1)}, bf16[1,512]{1,0:T(2,128)(2,1)}) custom-call(bf16[4,192,512]{2,1,0:T(8,128)(2,1)S(1)} %get-tuple-element.9.keys, bf16[4,192,512]{2,1,0:T(8,128)(2,1)S(1)} %get-tuple-element.10.values, bf16[1,512]{1,0:T(2,128)(2,1)S(1)} %get-tuple-element.11.mixed), custom_call_target="tpu_custom_call" | custom-call | tf_op jit(solution)/shard_map/pallas_call | solution.py:514

commit v5 on v4

--- a/solution.py
+++ b/solution.py
@@ -10,16 +10,17 @@
 
 MESH = pl.DeviceIdType.MESH
 MAP_ROWS = 16
+LANES = 128
 VMEM_BYTES = 67043328
 SMALL_BYTES = 16384
-SLICES = (3, 2, 2, 1)
+SLICES = (5, 2, 1)
 
 
 def kernel(
     n_sp, n_tp, heads, head_dim, chunk,
     x_ref, wk_ref, wv_ref, q_ref, lam_ref, gain_ref, wo_ref, fine_ref, coarse_ref,
     keys, values, mix_ref,
-    xg, wk, wv, wo, q, lam, gain, fine, coarse, stats, part, parts, sums,
+    xg, wk, wv, wo, q, lam, gain, fine, coarse, stats, part, parts, sums, turned_q, pick,
     load_sem, own_sem, up_sem, down_sem, near_send, near_recv, far_send, far_recv, twin_send, twin_recv,
     fwd_send, fwd_recv,
     wo_send, wo_recv, st_send, st_recv, pt_send, pt_recv,
@@ -74,6 +75,7 @@
         device_id_type=MESH,
     )
 
+    own_loads[0].start()
     barrier = pltpu.get_barrier_semaphore()
     for d in range(1, n_tp):
         pl.semaphore_signal(
@@ -90,7 +92,7 @@
     def _():
         pl.semaphore_signal(barrier, inc=1, device_id={"sp": sp + 1}, device_id_type=MESH)
 
-    for load in own_loads:
+    for load in own_loads[1:]:
         load.start()
     pl.semaphore_wait(barrier, n_tp - 1 + jnp.where(has_lower, 1, 0) + jnp.where(has_upper, 1, 0))
 
@@ -137,18 +139,25 @@
     lane = lax.broadcasted_iota(jnp.int32, (chunk, wide), 1)
     low_half = lax.rem(lane, head_dim) < head_dim // 2
 
+    def angles(block, j):
+        base = coarse[block * steps + j]
+        base_cos, base_sin = base[0:1, :], base[1:2, :]
+        cosine = base_cos * fine[0] - base_sin * fine[1]
+        sine = base_sin * fine[0] + base_cos * fine[1]
+        return cosine, sine
+
+    def swapped(raw):
+        ahead = pltpu.roll(raw, wide - head_dim // 2, 1)
+        behind = pltpu.roll(raw, head_dim // 2, 1)
+        return jnp.where(low_half, ahead, behind)
+
     def settle(block, first, count, raw_keys, raw_values):
         values[block, first * chunk:(first + count) * chunk, :] = raw_values.astype(jnp.bfloat16)
         for i in range(count):
-            base = coarse[block * steps + first + i]
-            base_cos, base_sin = base[0:1, :], base[1:2, :]
-            cosine = base_cos * fine[0] - base_sin * fine[1]
-            sine = base_sin * fine[0] + base_cos * fine[1]
+            cosine, sine = angles(block, first + i)
             for h in range(heads):
                 raw = raw_keys[i * chunk:(i + 1) * chunk, h * wide:(h + 1) * wide]
-                ahead = pltpu.roll(raw, wide - head_dim // 2, 1)
-                behind = pltpu.roll(raw, head_dim // 2, 1)
-                turned = raw * cosine + jnp.where(low_half, ahead, behind) * sine
+                turned = raw * cosine + swapped(raw) * sine
                 keys[
                     block, (first + i) * chunk:(first + i + 1) * chunk, h * wide:(h + 1) * wide
                 ] = turned.astype(jnp.bfloat16)
@@ -168,39 +177,59 @@
     map_col = lax.broadcasted_iota(jnp.int32, (MAP_ROWS, columns), 1) // head_dim
     spread = jnp.where(map_row == map_col, q[...].astype(jnp.float32), 0.0).astype(jnp.bfloat16)
 
-    def attend(state, blocks, first, count):
+    def weigh(highest, weight, rows_of_values):
+        total = jnp.sum(weight, axis=1, keepdims=True)
+        upper = weight.astype(jnp.bfloat16)
+        lower = (weight - upper.astype(jnp.float32)).astype(jnp.bfloat16)
+        read = jnp.dot(
+            jnp.concatenate([upper, lower], axis=0), rows_of_values,
+            preferred_element_type=jnp.float32,
+        )
+        return highest, total, read[:MAP_ROWS] + read[MAP_ROWS:]
+
+    def merge(one, two):
+        highest = jnp.maximum(one[0], two[0])
+        fades = jnp.exp(one[0] - highest), jnp.exp(two[0] - highest)
+        return (
+            highest,
+            one[1] * fades[0] + two[1] * fades[1],
+            one[2] * fades[0] + two[2] * fades[1],
+        )
+
+    def attend(state, block, first, count):
         where = slice(first * chunk, (first + count) * chunk)
-        scores = [
-            lax.dot_general(
-                spread, keys[block, where, :], (((1,), (1,)), ((), ())),
-                preferred_element_type=jnp.float32,
-            ) * head_dim ** (-0.5)
-            for block in blocks
-        ]
-        highest = functools.reduce(
-            jnp.maximum, [jnp.max(score, axis=1, keepdims=True) for score in scores]
-        )
-        if state is not None:
-            highest = jnp.maximum(highest, state[0])
-        total, read = 0.0, 0.0
-        for block, score in zip(blocks, scores):
-            weight = jnp.exp(score - highest)
-            total = total + jnp.sum(weight, axis=1, keepdims=True)
-            upper = weight.astype(jnp.bfloat16)
-            lower = (weight - upper.astype(jnp.float32)).astype(jnp.bfloat16)
-            both = jnp.dot(
-                jnp.concatenate([upper, lower], axis=0), values[block, where, :],
-                preferred_element_type=jnp.float32,
+        score = lax.dot_general(
+            spread, keys[block, where, :], (((1,), (1,)), ((), ())),
+            preferred_element_type=jnp.float32,
+        ) * head_dim ** (-0.5)
+        highest = jnp.max(score, axis=1, keepdims=True)
+        fresh = weigh(highest, jnp.exp(score - highest), values[block, where, :])
+        return fresh if state is None else merge(state, fresh)
+
+    def attend_raw(state, slots, raw_keys, raw_values):
+        products = jnp.concatenate(
+            [raw * turned_q[slot] for raw, slot in zip(raw_keys, slots)], axis=0
+        )
+        count = products.shape[0]
+        upper = products.astype(jnp.bfloat16)
+        lower = (products - upper.astype(jnp.float32)).astype(jnp.bfloat16)
+        score = jnp.dot(
+            jnp.concatenate([upper, lower], axis=0), pick[...], preferred_element_type=jnp.float32
+        )
+        score = score[:count] + score[count:]
+        highest = jnp.max(score, axis=0, keepdims=True)
+        room = -(-(count + 8) // LANES) * LANES - count
+        across = jnp.transpose(
+            jnp.concatenate(
+                [jnp.exp(score - highest), jnp.broadcast_to(highest, (room, LANES))], axis=0
             )
-            read = read + both[:MAP_ROWS] + both[MAP_ROWS:]
-        if state is not None:
-            fade = jnp.exp(state[0] - highest)
-            total = total + state[1] * fade
-            read = read + state[2] * fade
-        return highest, total, read
+        )[:MAP_ROWS]
+        rows_of_values = jnp.concatenate(raw_values, axis=0).astype(jnp.bfloat16)
+        fresh = weigh(across[:, count:count + 1], across[:, :count], rows_of_values)
+        return merge(state, fresh)
 
     project(tp, 0, steps)
-    state = attend(None, [tp], 0, steps)
+    state = attend(None, tp, 0, steps)
 
     pl.when(has_lower)(lambda: pl.semaphore_wait(up_sem, 1))
 
@@ -210,7 +239,7 @@
 
     near.wait_recv()
     project(partner, 0, steps)
-    state = attend(state, [partner], 0, steps)
+    state = attend(state, partner, 0, steps)
 
     pl.when(has_upper)(lambda: pl.semaphore_wait(down_sem, 1))
 
@@ -228,6 +257,20 @@
     sources = {d: lax.rem(partner + n_tp - 2 * d, n_tp) for d in range(1, chips)}
     others = {d: sources[d] + 1 - 2 * lax.rem(sources[d], 2) for d in sources}
     forwards = {}
+
+    pick_row = lax.broadcasted_iota(jnp.int32, (columns, LANES), 0) // head_dim
+    pick_lane = lax.broadcasted_iota(jnp.int32, (columns, LANES), 1)
+    pick[...] = jnp.where(pick_row == pick_lane, 1.0, 0.0).astype(jnp.bfloat16)
+    for d in sources:
+        for side, block in enumerate((sources[d], others[d])):
+            cosine, sine = angles(block, last)
+            for h in range(heads):
+                query = jnp.broadcast_to(
+                    q[0:1, h * wide:(h + 1) * wide].astype(jnp.float32), (chunk, wide)
+                )
+                turned_q[2 * (d - 1) + side, :, h * wide:(h + 1) * wide] = (
+                    query * cosine - swapped(query) * sine
+                ) * head_dim ** (-0.5)
 
     def forward(d, p):
         far[d, p].wait_recv()
@@ -245,35 +288,29 @@
         for d in sources:
             forward(d, j)
             project(sources[d], j, 1)
-            state = attend(state, [sources[d]], j, 1)
+            state = attend(state, sources[d], j, 1)
             forwards[d, j].wait_recv()
             project(others[d], j, 1)
-            state = attend(state, [others[d]], j, 1)
-
-    def add_slice(d, side, block, i):
-        raw_keys, raw_values = product(block, last, 1, cuts[i])
-        slot = 2 * (d - 1) + side
-        if i > 0:
-            raw_keys = raw_keys + sums[slot, :, :columns]
-            raw_values = raw_values + sums[slot, :, columns:]
-        sums[slot, :, :columns] = raw_keys
-        sums[slot, :, columns:] = raw_values
-
-    final = len(cuts) - 1
-    for i in range(final):
+            state = attend(state, others[d], j, 1)
+
+    tail = slice(edges[1], depth)
+
+    def add_first(slot, block):
+        sums[slot, :, :columns], sums[slot, :, columns:] = product(block, last, 1, cuts[0])
+
+    for d in sources:
+        forward(d, last)
+        add_first(2 * d - 2, sources[d])
+    for i in range(1, len(cuts) - 1):
         for d in sources:
             forward(d, last + i)
-            if i > 1:
-                forwards[d, last + i - 2].wait_recv()
-            add_slice(d, 0, sources[d], i)
-            if i > 1:
-                add_slice(d, 1, others[d], i - 2)
-    for i in range(max(final - 2, 0), final):
-        for d in sources:
-            forwards[d, last + i].wait_recv()
-            add_slice(d, 1, others[d], i)
+    for d in sources:
+        forwards[d, last].wait_recv()
+        add_first(2 * d - 1, others[d])
     for d in sources:
         pair = (sources[d], others[d])
+        for i in range(1, len(cuts) - 1):
+            forwards[d, last + i].wait_recv()
         for source in range(2):
             pltpu.make_async_remote_copy(
                 src_ref=piece_of(sources[d], len(pieces) - 1),
@@ -283,20 +320,17 @@
                 device_id={"tp": partner},
                 device_id_type=MESH,
             ).wait_recv()
-        piece = jnp.concatenate(
-            [xg[block, last * chunk:rows, cuts[final]] for block in pair], axis=0
-        )
-        raw_keys = jnp.dot(piece, wk[cuts[final], :], preferred_element_type=jnp.float32)
-        raw_values = jnp.dot(piece, wv[cuts[final], :], preferred_element_type=jnp.float32)
+        both = jnp.concatenate([xg[block, last * chunk:rows, tail] for block in pair], axis=0)
+        raws = []
+        for w, where in ((wk, slice(0, columns)), (wv, slice(columns, 2 * columns))):
+            raw = jnp.dot(both, w[tail, :], preferred_element_type=jnp.float32)
+            raws.append([
+                raw[side * chunk:(side + 1) * chunk] + sums[2 * (d - 1) + side, :, where]
+                for side in range(2)
+            ])
         for side, block in enumerate(pair):
-            slot = 2 * (d - 1) + side
-            part_of = slice(side * chunk, (side + 1) * chunk)
-            settle(
-                block, last, 1,
-                raw_keys[part_of] + sums[slot, :, :columns],
-                raw_values[part_of] + sums[slot, :, columns:],
-            )
-        state = attend(state, pair, last, 1)
+            settle(block, last, 1, raws[0][side], raws[1][side])
+        state = attend_raw(state, (2 * d - 2, 2 * d - 1), *raws)
 
     highest, total, read = state
     head_of = lax.broadcasted_iota(jnp.int32, (MAP_ROWS, wide), 0) // 2
@@ -485,6 +519,8 @@
             pltpu.VMEM((chips, 2, 8, out_cols), f32),
             pltpu.VMEM((chips, 8, out_cols), f32),
             pltpu.VMEM((2 * (chips - 1), chunk, 2 * columns), f32),
+            pltpu.VMEM((2 * (chips - 1), chunk, columns), f32),
+            pltpu.VMEM((columns, LANES), bf16),
             dma((9,)),
             dma((steps,)),
             pltpu.SemaphoreType.REGULAR,

time: 33.3 us -> 33.1 us (level)
  no operation moved by 1% of the time
where the time goes in v5:
time: 33.1 us; the launch traced here: 32.9 us
  Pallas kernels  32.3 us (98%)
  between operations  0.64 us (2%)
    pallas_call x1, Pallas kernels, on_device(): pl.pallas_call(functools.partial(kernel, n_sp, n_tp, heads, head_dim, chu...  31.1 us
    pallas_call x1, Pallas kernels, on_device(): pl.pallas_call(deliver, out_shape=(jax.ShapeDtypeStruct(cache, bf16), jax...  1.17 us

profile of v5, /device:TPU:0, one launch (start us, length us, event | category | flops | bytes accessed | tf_op | source)
XLA Modules:
  0.0 32.9 jit_solution(6131385871163550827)
XLA Ops:
  0.6 31.1 %shard_map.112 = (bf16[4,192,512]{2,1,0:T(8,128)(2,1)S(1)}, bf16[4,192,512]{2,1,0:T(8,128)(2,1)S(1)}, bf16[1,512]{1,0:T(2,128)(2,1)S(1)}) custom-call(bf16[1,192,2048]{2,1,0:T(8,128)(2,1)} %x_ref.1, bf16[2048,512]{1,0:T(8,128)(2,1)} %wk_ref.1, bf16[2048,512]{1,0:T(8,128)(2,1)} %wv_ref.1, bf16[1,512]{1,0:T(2,128)(2,1)} %q_ref.1, f32[1,4]{1,0:T(1,128)} %bitcast.4, ...), custom_call_target="tpu_custom_call" | custom-call | tf_op jit(solution)/shard_map/pallas_call | solution.py:499
  31.7 1.2 %shard_map.113 = (bf16[4,192,512]{2,1,0:T(8,128)(2,1)}, bf16[4,192,512]{2,1,0:T(8,128)(2,1)}, bf16[1,512]{1,0:T(2,128)(2,1)}) custom-call(bf16[4,192,512]{2,1,0:T(8,128)(2,1)S(1)} %get-tuple-element.9.keys, bf16[4,192,512]{2,1,0:T(8,128)(2,1)S(1)} %get-tuple-element.10.values, bf16[1,512]{1,0:T(2,128)(2,1)S(1)} %get-tuple-element.11.mixed), custom_call_target="tpu_custom_call" | custom-call | tf_op jit(solution)/shard_map/pallas_call | solution.py:550

commit v6 on v5

--- a/solution.py
+++ b/solution.py
@@ -14,6 +14,7 @@
 VMEM_BYTES = 67043328
 SMALL_BYTES = 16384
 SLICES = (5, 2, 1)
+RELAY_ROWS = 8
 
 
 def kernel(
@@ -21,8 +22,10 @@
     x_ref, wk_ref, wv_ref, q_ref, lam_ref, gain_ref, wo_ref, fine_ref, coarse_ref,
     keys, values, mix_ref,
     xg, wk, wv, wo, q, lam, gain, fine, coarse, stats, part, parts, sums, turned_q, pick,
+    relay_in, relay_out,
     load_sem, own_sem, up_sem, down_sem, near_send, near_recv, far_send, far_recv, twin_send, twin_recv,
     fwd_send, fwd_recv,
+    in_send, in_recv, out_send, out_recv, back_send, back_recv,
     wo_send, wo_recv, st_send, st_recv, pt_send, pt_recv,
 ):
     sp = lax.axis_index("sp")
@@ -92,36 +95,66 @@
     def _():
         pl.semaphore_signal(barrier, inc=1, device_id={"sp": sp + 1}, device_id_type=MESH)
 
+    @pl.when(sp == 0)
+    def _():
+        pl.semaphore_signal(barrier, inc=1, device_id={"sp": n_sp - 1}, device_id_type=MESH)
+
     for load in own_loads[1:]:
         load.start()
-    pl.semaphore_wait(barrier, n_tp - 1 + jnp.where(has_lower, 1, 0) + jnp.where(has_upper, 1, 0))
-
-    far = {}
-    for p in range(len(pieces) - 1):
-        if p < steps:
-            own_loads[p].wait()
+    pl.semaphore_wait(
+        barrier,
+        n_tp - 1 + jnp.where(has_lower, 1, 0) + jnp.where(has_upper, 1, 0)
+        + jnp.where(sp == n_sp - 1, 1, 0),
+    )
+
+    is_first, is_last = sp == 0, sp == n_sp - 1
+    relayed = last - 1
+    kept = chunk - RELAY_ROWS
+    relay_rows = pl.ds(relayed * chunk + kept, RELAY_ROWS)
+
+    def far_copy(d, p, count=chunk):
+        j, cut = pieces[p]
+        where = xg.at[tp, pl.ds(j * chunk, count), pl.ds(cut.start, cut.stop - cut.start)]
+        return pltpu.make_async_remote_copy(
+            src_ref=where,
+            dst_ref=where,
+            send_sem=far_send.at[d - 1, p],
+            recv_sem=far_recv.at[d - 1, p],
+            device_id={"tp": lax.rem(partner + 2 * d, n_tp)},
+            device_id_type=MESH,
+        )
+
+    def far_do(d, p, act):
+        if p == relayed:
+            pl.when(is_last)(lambda: act(far_copy(d, p, kept)))
+            pl.when(sp < n_sp - 1)(lambda: act(far_copy(d, p)))
+        else:
+            act(far_copy(d, p))
+
+    def start_far(p):
         for d in range(1, chips):
-            far[d, p] = pltpu.make_async_remote_copy(
-                src_ref=piece_of(tp, p),
-                dst_ref=piece_of(tp, p),
-                send_sem=far_send.at[d - 1, p],
-                recv_sem=far_recv.at[d - 1, p],
-                device_id={"tp": lax.rem(partner + 2 * d, n_tp)},
-                device_id_type=MESH,
-            )
-            far[d, p].start()
-    twins = {}
-    for d in range(1, chips):
-        for target in range(2):
-            twins[d, target] = pltpu.make_async_remote_copy(
-                src_ref=piece_of(tp, len(pieces) - 1),
-                dst_ref=piece_of(tp, len(pieces) - 1),
-                send_sem=twin_send.at[d - 1, target],
-                recv_sem=twin_recv.at[d - 1, core],
-                device_id={"tp": lax.rem(tp - core + 2 * d, n_tp) + target},
-                device_id_type=MESH,
-            )
-            twins[d, target].start()
+            far_do(d, p, lambda copy: copy.start())
+
+    to_first = pltpu.make_async_remote_copy(
+        src_ref=xg.at[tp, relay_rows],
+        dst_ref=relay_in,
+        send_sem=in_send,
+        recv_sem=in_recv,
+        device_id={"sp": 0},
+        device_id_type=MESH,
+    )
+    @pl.when(is_last)
+    def _():
+        own_loads[relayed].wait()
+        to_first.start()
+
+    for j in range(steps):
+        if j == relayed:
+            pl.when(sp < n_sp - 1)(own_loads[j].wait)
+        else:
+            own_loads[j].wait()
+        if j < relayed:
+            start_far(j)
     near = pltpu.make_async_remote_copy(
         src_ref=xg.at[tp],
         dst_ref=xg.at[tp],
@@ -134,7 +167,12 @@
     for load in loads:
         load.start()
     pl.when(is_lead)(own_wo.start)
-    pl.when(core == 0)(lent_wo.start)
+
+    pl.when(has_lower)(lambda: pl.semaphore_wait(up_sem, 1))
+
+    @pl.when(has_upper)
+    def _():
+        pl.semaphore_signal(up_sem, inc=1, device_id={"sp": sp + 1}, device_id_type=MESH)
 
     lane = lax.broadcasted_iota(jnp.int32, (chunk, wide), 1)
     low_half = lax.rem(lane, head_dim) < head_dim // 2
@@ -231,12 +269,6 @@
     project(tp, 0, steps)
     state = attend(None, tp, 0, steps)
 
-    pl.when(has_lower)(lambda: pl.semaphore_wait(up_sem, 1))
-
-    @pl.when(has_upper)
-    def _():
-        pl.semaphore_signal(up_sem, inc=1, device_id={"sp": sp + 1}, device_id_type=MESH)
-
     near.wait_recv()
     project(partner, 0, steps)
     state = attend(state, partner, 0, steps)
@@ -253,6 +285,26 @@
     lam_row = jnp.zeros((maps, wide), jnp.float32)
     for h in range(heads):
         lam_row = jnp.where(map_of == 2 * h, lam[0:1, h:h + 1], lam_row)
+
+    def relay_out_copy(d):
+        return pltpu.make_async_remote_copy(
+            src_ref=relay_in,
+            dst_ref=relay_out.at[d - 1],
+            send_sem=out_send.at[d - 1],
+            recv_sem=out_recv.at[d - 1],
+            device_id={"tp": lax.rem(partner + 2 * d, n_tp)},
+            device_id_type=MESH,
+        )
+
+    def relay_back_copy(d):
+        return pltpu.make_async_remote_copy(
+            src_ref=relay_out.at[d - 1],
+            dst_ref=xg.at[sources[d], relay_rows],
+            send_sem=back_send.at[d - 1],
+            recv_sem=back_recv.at[d - 1],
+            device_id={"sp": n_sp - 1},
+            device_id_type=MESH,
+        )
 
     sources = {d: lax.rem(partner + n_tp - 2 * d, n_tp) for d in range(1, chips)}
     others = {d: sources[d] + 1 - 2 * lax.rem(sources[d], 2) for d in sources}
@@ -273,7 +325,9 @@
                 ) * head_dim ** (-0.5)
 
     def forward(d, p):
-        far[d, p].wait_recv()
+        far_do(d, p, lambda copy: copy.wait_recv())
+        if p == relayed:
+            pl.when(is_last)(relay_back_copy(d).wait_recv)
         forwards[d, p] = pltpu.make_async_remote_copy(
             src_ref=piece_of(sources[d], p),
             dst_ref=piece_of(sources[d], p),
@@ -284,11 +338,46 @@
         )
         forwards[d, p].start()
 
+    twins = {}
+
+    def send_rest():
+        @pl.when(is_first)
+        def _():
+            to_first.wait_recv()
+            for d in range(1, chips):
+                relay_out_copy(d).start()
+
+        for p in range(relayed, len(pieces) - 1):
+            start_far(p)
+        for d in range(1, chips):
+            for target in range(2):
+                twins[d, target] = pltpu.make_async_remote_copy(
+                    src_ref=piece_of(tp, len(pieces) - 1),
+                    dst_ref=piece_of(tp, len(pieces) - 1),
+                    send_sem=twin_send.at[d - 1, target],
+                    recv_sem=twin_recv.at[d - 1, core],
+                    device_id={"tp": lax.rem(tp - core + 2 * d, n_tp) + target},
+                    device_id_type=MESH,
+                )
+                twins[d, target].start()
+
+    def hand_back():
+        @pl.when(is_first)
+        def _():
+            for d in sources:
+                relay_out_copy(d).wait_recv()
+                relay_back_copy(d).start()
+
     for j in range(last):
         for d in sources:
             forward(d, j)
             project(sources[d], j, 1)
             state = attend(state, sources[d], j, 1)
+            if d == chips - 1 and j == 0:
+                send_rest()
+            if d == chips - 1 and j == relayed - 1:
+                hand_back()
+                pl.when(core == 0)(lent_wo.start)
             forwards[d, j].wait_recv()
             project(others[d], j, 1)
             state = attend(state, others[d], j, 1)
@@ -446,7 +535,18 @@
         stats_copy(sp).wait_send()
 
     near.wait_send()
-    for copy in [*far.values(), *twins.values(), *forwards.values(), *exchanges]:
+    pl.when(is_last)(to_first.wait_send)
+
+    @pl.when(is_first)
+    def _():
+        for d in sources:
+            relay_out_copy(d).wait_send()
+            relay_back_copy(d).wait_send()
+
+    for d in sources:
+        for p in range(len(pieces) - 1):
+            far_do(d, p, lambda copy: copy.wait_send())
+    for copy in [*twins.values(), *forwards.values(), *exchanges]:
         copy.wait_send()
 
 
@@ -521,6 +621,8 @@
             pltpu.VMEM((2 * (chips - 1), chunk, 2 * columns), f32),
             pltpu.VMEM((2 * (chips - 1), chunk, columns), f32),
             pltpu.VMEM((columns, LANES), bf16),
+            pltpu.VMEM((RELAY_ROWS, depth), bf16),
+            pltpu.VMEM((chips - 1, RELAY_ROWS, depth), bf16),
             dma((9,)),
             dma((steps,)),
             pltpu.SemaphoreType.REGULAR,
@@ -535,6 +637,12 @@
             dma((chips - 1, pieces - 1)),
             dma,
             dma,
+            dma((chips - 1,)),
+            dma((chips - 1,)),
+            dma((chips - 1,)),
+            dma((chips - 1,)),
+            dma,
+            dma,
             dma((n_sp,)),
             dma((n_sp, 2)),
             dma((chips, 2)),

time: 33.1 us -> 32.8 us (level)
  no operation moved by 1% of the time
where the time goes in v6:
time: 32.8 us; the launch traced here: 32.6 us
  Pallas kernels  32 us (98%)
  between operations  0.64 us (2%)
    pallas_call x1, Pallas kernels, on_device(): pl.pallas_call(functools.partial(kernel, n_sp, n_tp, heads, head_dim, chu...  30.8 us
    pallas_call x1, Pallas kernels, on_device(): pl.pallas_call(deliver, out_shape=(jax.ShapeDtypeStruct(cache, bf16), jax...  1.17 us

profile of v6, /device:TPU:0, one launch (start us, length us, event | category | flops | bytes accessed | tf_op | source)
XLA Modules:
  0.0 32.6 jit_solution(14016488333138549229)
XLA Ops:
  0.6 30.8 %shard_map.112 = (bf16[4,192,512]{2,1,0:T(8,128)(2,1)S(1)}, bf16[4,192,512]{2,1,0:T(8,128)(2,1)S(1)}, bf16[1,512]{1,0:T(2,128)(2,1)S(1)}) custom-call(bf16[1,192,2048]{2,1,0:T(8,128)(2,1)} %x_ref.1, bf16[2048,512]{1,0:T(8,128)(2,1)} %wk_ref.1, bf16[2048,512]{1,0:T(8,128)(2,1)} %wv_ref.1, bf16[1,512]{1,0:T(2,128)(2,1)} %q_ref.1, f32[1,4]{1,0:T(1,128)} %bitcast.4, ...), custom_call_target="tpu_custom_call" | custom-call | tf_op jit(solution)/shard_map/pallas_call | solution.py:599
  31.5 1.2 %shard_map.113 = (bf16[4,192,512]{2,1,0:T(8,128)(2,1)}, bf16[4,192,512]{2,1,0:T(8,128)(2,1)}, bf16[1,512]{1,0:T(2,128)(2,1)}) custom-call(bf16[4,192,512]{2,1,0:T(8,128)(2,1)S(1)} %get-tuple-element.9.keys, bf16[4,192,512]{2,1,0:T(8,128)(2,1)S(1)} %get-tuple-element.10.values, bf16[1,512]{1,0:T(2,128)(2,1)S(1)} %get-tuple-element.11.mixed), custom_call_target="tpu_custom_call" | custom-call | tf_op jit(solution)/shard_map/pallas_call | solution.py:658

commit v7 on v6

--- a/solution.py
+++ b/solution.py
@@ -15,6 +15,7 @@
 SMALL_BYTES = 16384
 SLICES = (5, 2, 1)
 RELAY_ROWS = 8
+HELPER = 1
 
 
 def kernel(
@@ -95,7 +96,7 @@
     def _():
         pl.semaphore_signal(barrier, inc=1, device_id={"sp": sp + 1}, device_id_type=MESH)
 
-    @pl.when(sp == 0)
+    @pl.when(sp == HELPER)
     def _():
         pl.semaphore_signal(barrier, inc=1, device_id={"sp": n_sp - 1}, device_id_type=MESH)
 
@@ -107,7 +108,7 @@
         + jnp.where(sp == n_sp - 1, 1, 0),
     )
 
-    is_first, is_last = sp == 0, sp == n_sp - 1
+    is_helper, is_last = sp == HELPER, sp == n_sp - 1
     relayed = last - 1
     kept = chunk - RELAY_ROWS
     relay_rows = pl.ds(relayed * chunk + kept, RELAY_ROWS)
@@ -135,18 +136,18 @@
         for d in range(1, chips):
             far_do(d, p, lambda copy: copy.start())
 
-    to_first = pltpu.make_async_remote_copy(
+    to_helper = pltpu.make_async_remote_copy(
         src_ref=xg.at[tp, relay_rows],
         dst_ref=relay_in,
         send_sem=in_send,
         recv_sem=in_recv,
-        device_id={"sp": 0},
+        device_id={"sp": HELPER},
         device_id_type=MESH,
     )
     @pl.when(is_last)
     def _():
         own_loads[relayed].wait()
-        to_first.start()
+        to_helper.start()
 
     for j in range(steps):
         if j == relayed:
@@ -341,9 +342,9 @@
     twins = {}
 
     def send_rest():
-        @pl.when(is_first)
+        @pl.when(is_helper)
         def _():
-            to_first.wait_recv()
+            to_helper.wait_recv()
             for d in range(1, chips):
                 relay_out_copy(d).start()
 
@@ -362,7 +363,7 @@
                 twins[d, target].start()
 
     def hand_back():
-        @pl.when(is_first)
+        @pl.when(is_helper)
         def _():
             for d in sources:
                 relay_out_copy(d).wait_recv()
@@ -470,6 +471,21 @@
             device_id={"tp": 2 * chip + target},
             device_id_type=MESH,
         )
+
+    near.wait_send()
+    pl.when(is_last)(to_helper.wait_send)
+
+    @pl.when(is_helper)
+    def _():
+        for d in sources:
+            relay_out_copy(d).wait_send()
+            relay_back_copy(d).wait_send()
+
+    for d in sources:
+        for p in range(len(pieces) - 1):
+            far_do(d, p, lambda copy: copy.wait_send())
+    for copy in [*twins.values(), *forwards.values(), *exchanges]:
+        copy.wait_send()
 
     @pl.when(is_lead)
     def _():
@@ -526,28 +542,13 @@
 
     @pl.when(core == 0)
     def _():
+        lent_wo.wait_send()
+        stats_copy(sp).wait_send()
         mixed = None
         for d in range(chips):
             share_copy(d, 1).wait_recv()
             mixed = parts[d, 0:1] if mixed is None else mixed + parts[d, 0:1]
         mix_ref[...] = mixed.astype(jnp.bfloat16)
-        lent_wo.wait_send()
-        stats_copy(sp).wait_send()
-
-    near.wait_send()
-    pl.when(is_last)(to_first.wait_send)
-
-    @pl.when(is_first)
-    def _():
-        for d in sources:
-            relay_out_copy(d).wait_send()
-            relay_back_copy(d).wait_send()
-
-    for d in sources:
-        for p in range(len(pieces) - 1):
-            far_do(d, p, lambda copy: copy.wait_send())
-    for copy in [*twins.values(), *forwards.values(), *exchanges]:
-        copy.wait_send()
 
 
 def deliver(keys, values, mixed, key_out, value_out, mix_out, sem):
@@ -582,7 +583,7 @@
     head_dim = columns // (2 * heads)
     wide = 2 * head_dim
     seqs, rows, depth = x.shape
-    assert seqs == 1
+    assert seqs == 1 and n_sp > HELPER + 1
     chunk = rows // 4
     steps = rows // chunk
     chips = n_tp // 2

time: 32.8 us -> 32.4 us (0.988)
  Pallas kernels: 32 us -> 31.6 us
    pallas_call x1, Pallas kernels: 30.8 us -> 30.4 us  [on_device(): pl.pallas_call(functools.partial(kernel, n_sp, n_tp, heads, head_dim, chu...]
where the time goes in v7:
time: 32.4 us; the launch traced here: 32.2 us
  Pallas kernels  31.6 us (98%)
  between operations  0.64 us (2%)
    pallas_call x1, Pallas kernels, on_device(): pl.pallas_call(functools.partial(kernel, n_sp, n_tp, heads, head_dim, chu...  30.4 us
    pallas_call x1, Pallas kernels, on_device(): pl.pallas_call(deliver, out_shape=(jax.ShapeDtypeStruct(cache, bf16), jax...  1.17 us

profile of v7, /device:TPU:0, one launch (start us, length us, event | category | flops | bytes accessed | tf_op | source)
XLA Modules:
  0.0 32.2 jit_solution(4216205264604039195)
XLA Ops:
  0.6 30.4 %shard_map.112 = (bf16[4,192,512]{2,1,0:T(8,128)(2,1)S(1)}, bf16[4,192,512]{2,1,0:T(8,128)(2,1)S(1)}, bf16[1,512]{1,0:T(2,128)(2,1)S(1)}) custom-call(bf16[1,192,2048]{2,1,0:T(8,128)(2,1)} %x_ref.1, bf16[2048,512]{1,0:T(8,128)(2,1)} %wk_ref.1, bf16[2048,512]{1,0:T(8,128)(2,1)} %wv_ref.1, bf16[1,512]{1,0:T(2,128)(2,1)} %q_ref.1, f32[1,4]{1,0:T(1,128)} %bitcast.4, ...), custom_call_target="tpu_custom_call" | custom-call | tf_op jit(solution)/shard_map/pallas_call | solution.py:600
  31.0 1.2 %shard_map.113 = (bf16[4,192,512]{2,1,0:T(8,128)(2,1)}, bf16[4,192,512]{2,1,0:T(8,128)(2,1)}, bf16[1,512]{1,0:T(2,128)(2,1)}) custom-call(bf16[4,192,512]{2,1,0:T(8,128)(2,1)S(1)} %get-tuple-element.9.keys, bf16[4,192,512]{2,1,0:T(8,128)(2,1)S(1)} %get-tuple-element.10.values, bf16[1,512]{1,0:T(2,128)(2,1)S(1)} %get-tuple-element.11.mixed), custom_call_target="tpu_custom_call" | custom-call | tf_op jit(solution)/shard_map/pallas_call | solution.py:659

commit v8 on v7

--- a/solution.py
+++ b/solution.py
@@ -369,13 +369,12 @@
                 relay_out_copy(d).wait_recv()
                 relay_back_copy(d).start()
 
+    send_rest()
     for j in range(last):
         for d in sources:
             forward(d, j)
             project(sources[d], j, 1)
             state = attend(state, sources[d], j, 1)
-            if d == chips - 1 and j == 0:
-                send_rest()
             if d == chips - 1 and j == relayed - 1:
                 hand_back()
                 pl.when(core == 0)(lent_wo.start)

time: 32.4 us -> 32.4 us (level)
  no operation moved by 1% of the time
where the time goes in v8:
time: 32.4 us; the launch traced here: 32.2 us
  Pallas kernels  31.6 us (98%)
  between operations  0.64 us (2%)
    pallas_call x1, Pallas kernels, on_device(): pl.pallas_call(functools.partial(kernel, n_sp, n_tp, heads, head_dim, chu...  30.4 us
    pallas_call x1, Pallas kernels, on_device(): pl.pallas_call(deliver, out_shape=(jax.ShapeDtypeStruct(cache, bf16), jax...  1.17 us

profile of v8, /device:TPU:0, one launch (start us, length us, event | category | flops | bytes accessed | tf_op | source)
XLA Modules:
  0.0 32.2 jit_solution(11656912767364042737)
XLA Ops:
  0.6 30.4 %shard_map.112 = (bf16[4,192,512]{2,1,0:T(8,128)(2,1)S(1)}, bf16[4,192,512]{2,1,0:T(8,128)(2,1)S(1)}, bf16[1,512]{1,0:T(2,128)(2,1)S(1)}) custom-call(bf16[1,192,2048]{2,1,0:T(8,128)(2,1)} %x_ref.1, bf16[2048,512]{1,0:T(8,128)(2,1)} %wk_ref.1, bf16[2048,512]{1,0:T(8,128)(2,1)} %wv_ref.1, bf16[1,512]{1,0:T(2,128)(2,1)} %q_ref.1, f32[1,4]{1,0:T(1,128)} %bitcast.4, ...), custom_call_target="tpu_custom_call" | custom-call | tf_op jit(solution)/shard_map/pallas_call | solution.py:599
  31.1 1.2 %shard_map.113 = (bf16[4,192,512]{2,1,0:T(8,128)(2,1)}, bf16[4,192,512]{2,1,0:T(8,128)(2,1)}, bf16[1,512]{1,0:T(2,128)(2,1)}) custom-call(bf16[4,192,512]{2,1,0:T(8,128)(2,1)S(1)} %get-tuple-element.9.keys, bf16[4,192,512]{2,1,0:T(8,128)(2,1)S(1)} %get-tuple-element.10.values, bf16[1,512]{1,0:T(2,128)(2,1)S(1)} %get-tuple-element.11.mixed), custom_call_target="tpu_custom_call" | custom-call | tf_op jit(solution)/shard_map/pallas_call | solution.py:658
